TPU v7x, 256 devices: a whole 4x4x8 slice. The times are simulated.
256 devices in a mesh: ep: 32 (over z, x), tp: 8 (over y, core).
Axes of the slice: x: 4, y: 4, z: 8, core: 2. Of those that a mesh axis runs over, the one named last changes fastest.
Arguments:
- tokens: bfloat16 [512, 2048], P('ep'), may hold values from -6 to 6
- lengths: int32 [512], P('ep'), may hold values from 1024 to 16384
- old_state: float32 [512, 8, 128, 128], P('ep', 'tp'), may hold values from -2 to 2
- query_weight: bfloat16 [2048, 1024], P(None, 'tp'), may hold values from -0.125 to 0.125
- key_weight: bfloat16 [2048, 1024], P(None, 'tp'), may hold values from -0.125 to 0.125
- value_weight: bfloat16 [2048, 1024], P(None, 'tp'), may hold values from -0.125 to 0.125
- gate_weight: bfloat16 [2048, 1024], P(None, 'tp'), may hold values from -0.125 to 0.125
- head_gain: float32 [1024], P('tp'), may hold values from 0.1 to 1.9
- output_weight: bfloat16 [1024, 2048], P('tp'), may hold values from -0.1875 to 0.1875
- first_gain: float32 [2048], replicated, may hold values from 0.1 to 1.9
- expert_ids: int32 [512, 6], P('ep'), may hold values from 0 to 63, all different within a row; in each aligned block of 16 rows (0 to 15, 16 to 31, ...) at most 2 rows name the same one
- expert_weights: float32 [512, 6], P('ep'), may hold values from 0.05 to 0.8
- expert_gate: bfloat16 [64, 2048, 512], P('ep', None, 'tp'), may hold values from -0.125 to 0.125
- expert_up: bfloat16 [64, 2048, 512], P('ep', None, 'tp'), may hold values from -0.125 to 0.125
- expert_down: bfloat16 [64, 512, 2048], P('ep', 'tp'), may hold values from -0.25 to 0.25
- shared_gate: bfloat16 [2048, 512], P(None, 'tp'), may hold values from -0.125 to 0.125
- shared_up: bfloat16 [2048, 512], P(None, 'tp'), may hold values from -0.125 to 0.125
- shared_down: bfloat16 [512, 2048], P('tp'), may hold values from -0.25 to 0.25
- side_gate: bfloat16 [2048], replicated, may hold values from -0.125 to 0.125
- dense_gate: bfloat16 [2048, 8192], P(None, ('ep', 'tp')), may hold values from -0.125 to 0.125
- dense_up: bfloat16 [2048, 8192], P(None, ('ep', 'tp')), may hold values from -0.125 to 0.125
- dense_down: bfloat16 [8192, 2048], P(('ep', 'tp')), may hold values from -0.25 to 0.25
- second_gain: float32 [2048], replicated, may hold values from 0.1 to 1.9
Outputs:
- layer_out: bfloat16 [512, 2048], P('ep')
- new_state: float32 [512, 8, 128, 128], P('ep', 'tp')
Inputs may be any that keep to these rules, and one draw needn't show every extreme that they name: `expert_ids`: each row names 6 different experts. Among the 16 rows of one index of ep no expert is named by more than 2 rows, a bound that some block reaches.
All inputs are finite; a program needn't handle non-finite values.
Results may differ from a plain program's by a relative error of at most 0.017.
Values may be sent and summed in bfloat16 or wider, within the bound.
No kernel may reach another device: no remote copies, remote signals or barrier semaphores. Data moves between devices by JAX's collectives and lax.ppermute only.
A program may use at most 64 MiB of HBM per device.

v0:
```python
import jax
import jax.numpy as jnp
import numpy as np
from jax import lax
from jax.experimental import pallas as pl
from jax.experimental.pallas import tpu as pltpu
from jax.sharding import Mesh
from jax.sharding import PartitionSpec as P

HEADS = 8
EP = ("z", "x")
TP = ("y", "c")
ALL = ("z", "x", "y", "c")
NORM_EPS = 1e-05
RESIDUAL_SCALE = 2.0**0.5
BF = jnp.bfloat16
F32 = jnp.float32
VM = pl.BlockSpec(memory_space=pltpu.VMEM)
SM = pl.BlockSpec(memory_space=pltpu.SMEM)
HB = pl.BlockSpec(memory_space=pltpu.HBM)
NT = (((1,), (1,)), ((), ()))


def shifted(value, axis, step):
    n = lax.axis_size(axis)
    return lax.ppermute(value, axis, [(i, (i + step) % n) for i in range(n)])


def silu(v):
    return v / (1.0 + jnp.exp(-v))


def norm(inputs, gain):
    average = jnp.mean(inputs, axis=-1, keepdims=True)
    centered = inputs - average
    variance = jnp.mean(centered * centered, axis=-1, keepdims=True)
    return centered * lax.rsqrt(variance + NORM_EPS) * gain


def dot(a, b):
    return jnp.dot(a, b, preferred_element_type=F32)


def dot_nt(a, b):
    return lax.dot_general(a, b, NT, preferred_element_type=F32)


def columns_of(rows):
    n = rows.shape[0]
    return jnp.concatenate([rows, jnp.zeros((128 - n, 128), F32)], axis=0).T


def decay_row():
    head = (lax.axis_index("y") * 2 + lax.axis_index("c")).astype(F32)
    return 1.0 - jnp.exp2(-2.0 - 10.0 * jnp.full((1, 128), head, F32) / (HEADS - 1))


def mixer_kernel(
    lengths, frequency, tokens, gain, wq, wk, wv, wg, state, ow, ed, dd, sd,
    kept, given, key_out, value_out, d0, d1, d2, d3,
    bq, bk, bv, bg, bs, bo, rows, sems, dsems,
):
    moves = [
        pltpu.make_async_copy(src, dst, sems.at[i])
        for i, (src, dst) in enumerate(
            ((wq, bq), (wk, bk), (state, bs), (wv, bv), (wg, bg), (ow, bo))
        )
    ]
    for move in moves:
        move.start()
    slices = []
    for k, out in enumerate((d0, d1, d2, d3)):
        cols = pl.ds(pl.multiple_of(lax.rem(lax.axis_index("y") + k, 4) * 512, 512), 512)
        for src, dst in (
            (ed.at[0, :, cols], out.at[pl.ds(0, 64)]),
            (ed.at[1, :, cols], out.at[pl.ds(64, 64)]),
            (sd.at[:, cols], out.at[pl.ds(128, 64)]),
            (dd.at[:, cols], out.at[pl.ds(192, 32)]),
        ):
            c = pltpu.make_async_copy(src, dst, dsems.at[len(slices)])
            c.start()
            slices.append(c)
    f = frequency[...]
    for i in range(16):
        rows[i : i + 1, :] = jnp.full((1, 128), lengths[i].astype(F32), F32) * f
    angles = rows[...]
    lane = lax.broadcasted_iota(jnp.int32, (16, 128), 1)
    cos2 = jnp.cos(angles)
    sin2 = jnp.sin(angles) * jnp.where(lane < 64, -1.0, 1.0)
    decay = decay_row()
    t = tokens[...]

    def turned(v):
        return v * cos2 + pltpu.roll(v, 64, 1) * sin2

    moves[0].wait()
    q = turned(dot(t, bq[...]))
    qc = columns_of(q)
    moves[1].wait()
    k = turned(dot(t, bk[...]) * 128 ** (-0.5))
    key_out[...] = k
    moves[2].wait()
    for i in range(16):
        rows[i : i + 1, :] = jnp.sum(qc[:, i : i + 1] * bs[i], axis=0, keepdims=True)
    moves[3].wait()
    v = dot(t, bv[...])
    value_out[...] = v
    moves[4].wait()
    g = dot(t, bg[...])
    match = jnp.sum(q * k, axis=1, keepdims=True)
    readout = decay * rows[...] + match * v
    mixed = (norm(readout, gain[...]) * silu(g)).astype(BF)
    moves[5].wait()
    partial = dot(mixed, bo[...])
    low, high = partial[:8], partial[8:]
    first = lax.axis_index("c") == 0
    kept[...] = jnp.where(first, low, high).astype(BF)
    given[...] = jnp.where(first, high, low).astype(BF)
    for c in slices:
        c.wait()


def pack_kernel(*refs):
    own, peer, w_out, sems = refs[0:6], refs[6:12], refs[12], refs[13]
    moves = []

    def move(src, dst):
        c = pltpu.make_async_copy(src, dst, sems.at[len(moves)])
        c.start()
        moves.append(c)

    for side, (eg, eu, dg, du, sg, su) in enumerate((own, peer)):
        for half, (e, d, s) in enumerate(((eg, dg, sg), (eu, du, su))):
            o = 512 * side + 256 * half
            move(e.at[0], w_out.at[pl.ds(o, 64)])
            move(e.at[1], w_out.at[pl.ds(o + 64, 64)])
            move(d, w_out.at[pl.ds(o + 128, 32)])
            move(s, w_out.at[pl.ds(o + 160, 64)])
            move(d, w_out.at[pl.ds(o + 224, 32)])
    for c in moves:
        c.wait()


def arrange_kernel(y0, y1, y2, y3, p0, p1, p2, p3, out):
    for k, pair in enumerate(((y0, p0), (y1, p1), (y2, p2), (y3, p3))):
        for s, src in enumerate(pair):
            for j in range(3):
                o = 512 * j + 128 * k + 64 * s
                out[o : o + 64, :] = src[64 * j : 64 * j + 64, :]
            o = 1536 + 64 * k + 32 * s
            out[o : o + 32, :] = src[192:224, :]


def state_kernel(keys, values, state, new_state, bs, bn, sems):
    load = pltpu.make_async_copy(state, bs, sems.at[0])
    load.start()
    kc = columns_of(keys[...])
    decay = decay_row()
    load.wait()
    for i in range(16):
        bn[i] = decay * bs[i] + kc[:, i : i + 1] * values[i : i + 1, :]
    store = pltpu.make_async_copy(bn, new_state, sems.at[1])
    store.start()
    store.wait()


def after_kernel(pair, r1, r2, r3, tokens, gain, ids, ews, after, sent, table):
    first = lax.axis_index("c") == 0
    table[...] = jnp.zeros((128, 128), F32)
    w = ews[...]
    high = w.astype(BF).astype(F32)
    table[0:6, 0:16] = ids[...].astype(F32)
    table[8:14, 0:16] = high
    table[16:22, 0:16] = w - high
    f = table[...].T
    f = jnp.where(first, f[0:8], f[8:16]).astype(BF)
    t = tokens[...].astype(F32)
    mine = jnp.where(first, t[:8], t[8:])
    branch = pair[...].astype(F32)
    for r in (r1, r2, r3):
        branch = branch + r[...].astype(F32)
    a = norm(RESIDUAL_SCALE * mine + branch, gain[...]).astype(BF)
    after[...] = a
    for j in range(8):
        sent[j, :, 0:2048] = a
        sent[j, :, 2048:2176] = f


def hidden_kernel(b0, b1, b2, b3, w_all, side, h_out, pt_out, acts, info, xo, xp):
    for k, b in enumerate((b0, b1, b2, b3)):
        acts[64 * k : 64 * k + 64, :] = b[:, 0:2048]
        info[64 * k : 64 * k + 64, :] = b[:, 2048:2176].astype(F32)
    a = acts[...]
    lane = lax.broadcasted_iota(jnp.int32, (256, 128), 1)
    row = lax.broadcasted_iota(jnp.int32, (256, 128), 0)
    f = info[...]
    w = pltpu.roll(f, 128 - 8, 1) + pltpu.roll(f, 128 - 16, 1)
    zi = lax.axis_index("z")
    e0 = ((zi * 4 + lax.axis_index("x")) * 2).astype(F32)
    named = lane < 6
    m0 = jnp.logical_and(f == e0, named)
    m1 = jnp.logical_and(f == e0 + 1.0, named)
    s0 = jnp.sum(jnp.where(m0, w, 0.0), axis=1, keepdims=True)
    s1 = jnp.sum(jnp.where(m1, w, 0.0), axis=1, keepdims=True)
    a0 = jnp.sum(jnp.where(m0, 1.0, 0.0), axis=1, keepdims=True)
    a1 = jnp.sum(jnp.where(m1, 1.0, 0.0), axis=1, keepdims=True)
    flags = jnp.where(lane == 0, a0, jnp.where(lane == 1, a1, 0.0)).astype(BF)
    r2 = lax.broadcasted_iota(jnp.int32, (256, 256), 0)
    c2 = lax.broadcasted_iota(jnp.int32, (256, 256), 1)
    earlier = jnp.logical_and((r2 >> 3) == (c2 >> 3), c2 < r2)
    rank = dot(jnp.where(earlier, 1.0, 0.0).astype(BF), flags)
    base = ((row >> 3) * 2).astype(F32)
    lane_f = lane.astype(F32)
    t0 = jnp.logical_and(a0 > 0.5, base + rank[:, 0:1] == lane_f)
    t1 = jnp.logical_and(a1 > 0.5, base + rank[:, 1:2] == lane_f - 64.0)
    pt = jnp.where(jnp.where(lane < 64, jnp.where(t0, 1.0, 0.0), jnp.where(t1, 1.0, 0.0)) > 0.5, 1.0, 0.0)
    pt_out[...] = pt.astype(BF)
    pm = pt.T.astype(BF)

    switch = 1.0 / (1.0 + jnp.exp(-dot_nt(a, side[...])[:, 0:1]))
    share = jnp.where(lane < 64, s0, s1)

    def hidden_of(start, tail):
        gate = dot_nt(a, w_all[start : start + 256, :])
        up = dot_nt(a, w_all[start + 256 : start + 512, :])
        h = silu(gate) * up
        x = h[:, 128:256]
        tail[...] = x
        return (h[:, 0:128] * share).astype(BF), x * switch

    ho, do = hidden_of(0, xo)
    hp, dp = hidden_of(512, xp)
    eo = dot(pm, ho)
    ep = dot(pm, hp)
    lane1 = lane[:128]
    row1 = row[:128]
    near = lane1 < 64
    upper = jnp.where(near, eo, pltpu.roll(ep, 64, 1))
    lower = jnp.where(near, pltpu.roll(eo, 64, 1), ep)
    h_out[128:256, :] = jnp.where(row1 < 64, upper, lower).astype(BF)
    dense = jnp.where(lane < 32, do, pltpu.roll(dp, 32, 1))
    h_out[0:128, :] = jnp.where(near, dense[0:128], pltpu.roll(dense[128:256], 64, 1)).astype(BF)
    mine = pl.ds(pl.multiple_of(zi * 8, 8), 8)
    so, sp = xo[mine, :], xp[mine, :]
    s = jnp.where(lane[:8] < 64, pltpu.roll(so, 96, 1), pltpu.roll(sp, 32, 1))
    h_out[256:272, :] = jnp.concatenate([s, jnp.zeros((8, 128), F32)], axis=0).astype(BF)


def down_kernel(h0, h1, h2, h3, pt, d_all, out, shared):
    hs = (h0, h1, h2, h3)
    near = lax.broadcasted_iota(jnp.int32, (128, 128), 1) < 64
    total = None
    for n in range(2):
        u = hs[2 * n][0:128, :].astype(F32)
        v = hs[2 * n + 1][0:128, :].astype(F32)
        top = jnp.where(near, u, pltpu.roll(v, 64, 1))
        bottom = jnp.where(near, pltpu.roll(u, 64, 1), v)
        h = jnp.concatenate([top, bottom], axis=0).astype(BF)
        part = dot(h, d_all[1536 + 128 * n : 1664 + 128 * n, :])
        total = part if total is None else total + part
    outs = []
    for e in range(2):
        h = jnp.concatenate([r[128 + 64 * e : 192 + 64 * e, :] for r in hs], axis=1)
        outs.append(dot(h, d_all[512 * e : 512 * e + 512, :]))
    total = total + dot(pt[...], jnp.concatenate(outs, axis=0).astype(BF))
    h = jnp.concatenate([r[256:272, :] for r in hs], axis=1)
    shared[...] = dot(h, d_all[1024:1536, :])[0:8]
    for k in range(4):
        block = total[64 * k : 64 * k + 64].astype(BF).reshape(8, 8, 512)
        out[:, lax.rem(lax.axis_index("x") + 4 - k, 4)] = block


def sum_kernel(back, shared, out):
    total = shared[...]
    for j in range(32):
        total = total + back[j].astype(F32)
    for j in range(8):
        out[j] = total


def last_kernel(got, own, other, gain, out):
    first = lax.axis_index("c") == 0
    mine, theirs = own[...].astype(F32), other[...].astype(F32)
    low = jnp.where(first, mine, theirs)
    high = jnp.where(first, theirs, mine)
    rows = []
    for c, residual in enumerate((low, high)):
        side = jnp.concatenate([got[2 * y + c] for y in range(4)], axis=1)
        rows.append(norm(RESIDUAL_SCALE * residual + side, gain[...]))
    out[...] = jnp.concatenate(rows, axis=0).astype(BF)


def limit(mib):
    return pltpu.CompilerParams(vmem_limit_bytes=mib * 2**20)


def shape(*dims, dtype=BF):
    return pltpu.VMEM(dims, dtype)


def near(value):
    return pltpu.with_memory_space_constraint(value, pltpu.VMEM)


def big(value):
    return pltpu.with_memory_space_constraint(value, pltpu.HBM)


def layer(
    tokens,
    lengths,
    old_state,
    query_weight,
    key_weight,
    value_weight,
    gate_weight,
    head_gain,
    output_weight,
    first_gain,
    expert_ids,
    expert_weights,
    expert_gate,
    expert_up,
    expert_down,
    shared_gate,
    shared_up,
    shared_down,
    side_gate,
    dense_gate,
    dense_up,
    dense_down,
    second_gain,
):
    frequency = np.asarray(1.0 / 10000.0 ** ((np.arange(128) % 64) / 64.0), np.float32)
    state = old_state.reshape(16, 128, 128)
    kept, given, keys, values, *downs = pl.pallas_call(
        mixer_kernel,
        in_specs=[SM, VM, VM, VM] + [HB] * 9,
        out_specs=[VM] * 8,
        out_shape=[shape(8, 2048)] * 2 + [shape(16, 128, dtype=F32)] * 2 + [shape(224, 512)] * 4,
        scratch_shapes=[pltpu.VMEM((2048, 128), BF)] * 4
        + [
            pltpu.VMEM((16, 128, 128), F32),
            pltpu.VMEM((128, 2048), BF),
            pltpu.VMEM((16, 128), F32),
            pltpu.SemaphoreType.DMA((6,)),
            pltpu.SemaphoreType.DMA((16,)),
        ],
        compiler_params=limit(8),
        name="mixer",
    )(
        big(lengths), big(jnp.asarray(frequency)[None]), big(tokens), big(head_gain.reshape(1, 128)),
        big(query_weight), big(key_weight), big(value_weight), big(gate_weight), big(state),
        big(output_weight), big(expert_down), big(dense_down), big(shared_down),
    )

    pair = (kept.astype(F32) + shifted(given, "c", 1).astype(F32)).astype(BF)
    raw = (
        expert_gate.transpose(0, 2, 1), expert_up.transpose(0, 2, 1),
        dense_gate.T, dense_up.T, shared_gate.T, shared_up.T,
    )
    side = jnp.broadcast_to(side_gate[None], (8, 2048))
    raw, side, pair = lax.optimization_barrier((raw, side, pair))
    arrived = [shifted(pair, "y", k) for k in range(1, 4)]
    peers = [shifted(r, "c", 1) for r in raw]
    after, sent = pl.pallas_call(
        after_kernel,
        in_specs=[VM] * 8,
        out_specs=[VM, VM],
        out_shape=[shape(8, 2048), jax.ShapeDtypeStruct((8, 8, 2176), BF)],
        scratch_shapes=[pltpu.VMEM((128, 128), F32)],
        compiler_params=limit(4),
        name="after",
    )(
        pair, *arrived, big(tokens), big(first_gain.reshape(1, 2048)),
        big(expert_ids.T), big(expert_weights.T),
    )

    peers, downs, side, sent = lax.optimization_barrier((peers, downs, side, sent))
    block = lax.all_to_all(sent, "z", 0, 0, tiled=True).reshape(64, 2176)
    from_y = [downs[0]] + [shifted(downs[k], "y", k) for k in range(1, 4)]
    blocks = [block] + [shifted(block, "x", k) for k in range(1, 4)]
    other = shifted(after, "c", 1)
    from_c = [shifted(d, "c", 1) for d in from_y]
    w_all = pl.pallas_call(
        pack_kernel,
        in_specs=[HB] * 12,
        out_specs=VM,
        out_shape=shape(1024, 2048),
        scratch_shapes=[pltpu.SemaphoreType.DMA((20,))],
        compiler_params=limit(2),
        name="pack",
    )(*[big(v) for v in raw], *peers)
    new_state = pl.pallas_call(
        state_kernel,
        in_specs=[VM, VM, HB],
        out_specs=HB,
        out_shape=pltpu.HBM((16, 128, 128), F32),
        scratch_shapes=[
            pltpu.VMEM((16, 128, 128), F32),
            pltpu.VMEM((16, 128, 128), F32),
            pltpu.SemaphoreType.DMA((2,)),
        ],
        compiler_params=limit(4),
        name="state",
    )(keys, values, big(state))

    hidden, slots = pl.pallas_call(
        hidden_kernel,
        in_specs=[VM] * 6,
        out_specs=[VM] * 2,
        out_shape=[shape(272, 128), shape(256, 128)],
        scratch_shapes=[
            pltpu.VMEM((256, 2048), BF),
            pltpu.VMEM((256, 128), F32),
            pltpu.VMEM((256, 128), F32),
            pltpu.VMEM((256, 128), F32),
        ],
        compiler_params=limit(8),
        name="hidden",
    )(*blocks, near(w_all), side)
    gathered = [hidden] + [shifted(hidden, "y", k) for k in range(1, 4)]
    d_all = pl.pallas_call(
        arrange_kernel,
        in_specs=[VM] * 8,
        out_specs=VM,
        out_shape=shape(1792, 512),
        compiler_params=limit(2),
        name="arrange",
    )(*from_y, *from_c)
    partial, shared = pl.pallas_call(
        down_kernel,
        in_specs=[VM] * 6,
        out_specs=[VM, VM],
        out_shape=[shape(8, 4, 8, 512), shape(8, 512, dtype=F32)],
        compiler_params=limit(6),
        name="down",
    )(*gathered, slots, near(d_all))

    back = lax.all_to_all(partial.reshape(32, 8, 512), EP, 0, 0, tiled=True)
    mine = pl.pallas_call(
        sum_kernel,
        in_specs=[VM, VM],
        out_specs=VM,
        out_shape=jax.ShapeDtypeStruct((8, 8, 512), F32),
        compiler_params=limit(3),
        name="sum",
    )(back, shared)
    got = lax.all_to_all(mine, TP, 0, 0, tiled=True)
    layer_out = pl.pallas_call(
        last_kernel,
        in_specs=[VM] * 4,
        out_specs=VM,
        out_shape=jax.ShapeDtypeStruct((16, 2048), BF),
        compiler_params=limit(3),
        name="last",
    )(got, after, other, big(second_gain.reshape(1, 2048)))
    return (layer_out, new_state.reshape(16, 1, 128, 128))


def solution(mesh):
    finer = Mesh(mesh.devices.reshape(8, 4, 4, 2), ALL)
    return jax.shard_map(
        layer,
        mesh=finer,
        in_specs=(
            P(EP, None),
            P(EP),
            P(EP, TP, None, None),
            P(None, TP),
            P(None, TP),
            P(None, TP),
            P(None, TP),
            P(TP),
            P(TP, None),
            P(),
            P(EP, None),
            P(EP, None),
            P(EP, None, TP),
            P(EP, None, TP),
            P(EP, TP, None),
            P(None, TP),
            P(None, TP),
            P(TP, None),
            P(),
            P(None, ALL),
            P(None, ALL),
            P(ALL, None),
            P(),
        ),
        out_specs=(P(EP, None), P(EP, TP, None, None)),
        check_vma=False,
    )
```

profile of v0, /device:TPU:1, one launch (start us, length us, event | category | flops | bytes accessed | tf_op | source)
XLA Modules:
  0.0 96.5 jit_solution(14548035562242952843)
XLA Ops:
  0.6 0.0 copy-start
  0.6 0.0 copy-start.1
  0.7 0.0 copy-start.4
  0.7 0.0 copy-start.5
  0.7 0.0 copy-start.2
  0.7 0.0 copy-start.3
  0.7 4.9 %mixer.1 = (bf16[8,2048]{1,0:T(8,128)(2,1)S(1)}, bf16[8,2048]{1,0:T(8,128)(2,1)S(1)}, f32[16,128]{1,0:T(8,128)S(1)}, f32[16,128]{1,0:T(8,128)S(1)}, bf16[224,512...) custom-call(s32[16]{0:T(128)} %lengths.1, ...), custom_call_target="tpu_custom_call" | custom-call | tf_op jit(solution)/shard_map/mixer/pallas_call | solution.py:336
  5.7 3.3 %collective-permute-start = (bf16[8,2048]{1,0:T(8,128)(2,1)S(1)}, bf16[8,2048]{1,0:T(8,128)(2,1)S(1)}, u32[]{:S(2)}, u32[]{:S(2)}) collective-permute-start(bf16[8,2048]{1,0:T(8,128)(2,1)S(1)} %get-tuple-element.37), channel_id=1, source_target_pairs={{0,1},{1,0},{2,3},{3,2},{4,5},{5,4},{6,7},{7,6},{8,9},{9,8},{10,11... | collective-permute-start | bytes 98312 | tf_op jit(solution)/shard_map/ppermute | solution.py:26
  8.9 0.9 collective-permute-done
  9.8 0.4 collective-permute-start.1
  10.3 0.2 collective-permute-start.2
  10.5 2.2 %collective-permute-start.8 = (bf16[8,2048]{1,0:T(8,128)(2,1)S(1)}, bf16[8,2048]{1,0:T(8,128)(2,1)S(1)}, u32[]{:S(2)}, u32[]{:S(2)}) collective-permute-start(bf16[8,2048]{1,0:T(8,128)(2,1)S(1)} %add_convert_fusion.pair), channel_id=1, source_target_pairs={{0,4},{2,6},{4,0},{6,2},{1,5},{3,7},{5,1},{7,3},{8,12},{10,14},{12... | collective-permute-start | bytes 98312 | tf_op jit(solution)/shard_map/ppermute | solution.py:26
  12.7 1.1 %collective-permute-start.9 = (bf16[8,2048]{1,0:T(8,128)(2,1)S(1)}, bf16[8,2048]{1,0:T(8,128)(2,1)S(1)}, u32[]{:S(2)}, u32[]{:S(2)}) collective-permute-start(bf16[8,2048]{1,0:T(8,128)(2,1)S(1)} %add_convert_fusion.pair), channel_id=1, source_target_pairs={{0,6},{2,0},{4,2},{6,4},{1,7},{3,1},{5,3},{7,5},{8,14},{10,8},{12,... | collective-permute-start | bytes 98312 | tf_op jit(solution)/shard_map/ppermute | solution.py:26
  13.7 0.7 collective-permute-done.7.r1
  14.4 1.9 %collective-permute-start.3 = (bf16[32,2048]{1,0:T(8,128)(2,1)S(1)}, bf16[32,2048]{1,0:T(8,128)(2,1)S(1)}, u32[]{:S(2)}, u32[]{:S(2)}) collective-permute-start(bf16[32,2048]{1,0:T(8,128)(2,1)S(1)} %bitcast.34), channel_id=1, source_target_pairs={{0,1},{1,0},{2,3},{3,2},{4,5},{5,4},{6,7},{7,6},{8,9},{9,8},{10,11... | collective-permute-start | bytes 393224 | tf_op jit(solution)/shard_map/ppermute | solution.py:26
  16.4 0.1 collective-permute-start.5
  16.5 1.0 %collective-permute-start.6 = (bf16[64,2048]{1,0:T(8,128)(2,1)S(1)}, bf16[64,2048]{1,0:T(8,128)(2,1)S(1)}, u32[]{:S(2)}, u32[]{:S(2)}) collective-permute-start(bf16[64,2048]{1,0:T(8,128)(2,1)S(1)} %bitcast.32), channel_id=1, source_target_pairs={{0,1},{1,0},{2,3},{3,2},{4,5},{5,4},{6,7},{7,6},{8,9},{9,8},{10,11... | collective-permute-start | bytes 786440 | tf_op jit(solution)/shard_map/ppermute | solution.py:26
  17.5 0.2 collective-permute-start.4
  17.7 1.8 %after.1 = (bf16[8,2048]{1,0:T(8,128)(2,1)S(1)}, bf16[8,8,2176]{2,1,0:T(8,128)(2,1)}) custom-call(bf16[8,2048]{1,0:T(8,128)(2,1)S(1)} %add_convert_fusion.pair, bf16[8,2048]{1,0:T(8,128)(2,1)S(1)} %collective-permute-done.7.r1, bf16[8,2048]{1,0:T(8,128)(2,1)S(1)} %collective-permute-done.8.r2, bf16[8,2048]{1,0:T(8,128)(2,1)S(1)} %collective-permute-done.9.r3, ...), custom_call_target="tpu_custom_call" | custom-call | tf_op jit(solution)/shard_map/after/pallas_call | solution.py:366
  19.5 8.1 %all-to-all-start = ((bf16[8,8,2176]{2,1,0:T(8,128)(2,1)}), bf16[8,8,2176]{2,1,0:T(8,128)(2,1)S(1)}, u32[]{:S(2)}, u32[]{:S(2)}) async-start(bf16[8,8,2176]{2,1,0:T(8,128)(2,1)} %get-tuple-element.51), calls=%async_computation | async-start | bytes 557056 | tf_op jit(solution)/shard_map/all_to_all | solution.py:380
  27.6 0.3 collective-permute-start.16
  27.9 3.1 %collective-permute-start.17 = (bf16[224,512]{1,0:T(8,128)(2,1)}, bf16[224,512]{1,0:T(8,128)(2,1)S(1)}, u32[]{:S(2)}, u32[]{:S(2)}) collective-permute-start(bf16[224,512]{1,0:T(8,128)(2,1)} %get-tuple-element.63), channel_id=1, source_target_pairs={{0,4},{2,6},{4,0},{6,2},{1,5},{3,7},{5,1},{7,3},{8,12},{10,14},{12... | collective-permute-start | bytes 688136 | tf_op jit(solution)/shard_map/ppermute | solution.py:26
  31.1 0.3 collective-permute-start.18
  31.3 7.8 %all-to-all-done = bf16[8,8,2176]{2,1,0:T(8,128)(2,1)S(1)} async-done(((bf16[8,8,2176]{2,1,0:T(8,128)(2,1)}), bf16[8,8,2176]{2,1,0:T(8,128)(2,1)S(1)}, u32[]{:S(2)}, u32[]{:S(2)}) %all-to-all-start) | async-done | bytes 278560 | tf_op jit(solution)/shard_map/all_to_all | solution.py:380
  39.2 1.2 %collective-permute-start.10 = (bf16[64,2176]{1,0:T(8,128)(2,1)S(1)}, bf16[64,2176]{1,0:T(8,128)(2,1)S(1)}, u32[]{:S(2)}, u32[]{:S(2)}) collective-permute-start(bf16[64,2176]{1,0:T(8,128)(2,1)S(1)} %bitcast.17), channel_id=1, source_target_pairs={{0,8},{8,16},{16,24},{24,0},{1,9},{9,17},{17,25},{25,1},{2,10},{10... | collective-permute-start | bytes 835592 | tf_op jit(solution)/shard_map/ppermute | solution.py:26
  40.4 2.5 %collective-permute-start.11 = (bf16[64,2176]{1,0:T(8,128)(2,1)S(1)}, bf16[64,2176]{1,0:T(8,128)(2,1)S(1)}, u32[]{:S(2)}, u32[]{:S(2)}) collective-permute-start(bf16[64,2176]{1,0:T(8,128)(2,1)S(1)} %bitcast.18), channel_id=1, source_target_pairs={{0,16},{8,24},{16,0},{24,8},{1,17},{9,25},{17,1},{25,9},{2,18},{10... | collective-permute-start | bytes 835592 | tf_op jit(solution)/shard_map/ppermute | solution.py:26
  42.8 1.2 %collective-permute-start.12 = (bf16[64,2176]{1,0:T(8,128)(2,1)S(1)}, bf16[64,2176]{1,0:T(8,128)(2,1)S(1)}, u32[]{:S(2)}, u32[]{:S(2)}) collective-permute-start(bf16[64,2176]{1,0:T(8,128)(2,1)S(1)} %bitcast.19), channel_id=1, source_target_pairs={{0,24},{8,0},{16,8},{24,16},{1,25},{9,1},{17,9},{25,17},{2,26},{10... | collective-permute-start | bytes 835592 | tf_op jit(solution)/shard_map/ppermute | solution.py:26
  44.0 2.5 %collective-permute-start.19 = (bf16[224,512]{1,0:T(8,128)(2,1)S(1)}, bf16[224,512]{1,0:T(8,128)(2,1)S(1)}, u32[]{:S(2)}, u32[]{:S(2)}) collective-permute-start(bf16[224,512]{1,0:T(8,128)(2,1)S(1)} %get-tuple-element.61.y0), channel_id=1, source_target_pairs={{0,1},{1,0},{2,3},{3,2},{4,5},{5,4},{6,7},{7,6},{8,9},{9,8},{10,11... | collective-permute-start | bytes 688136 | tf_op jit(solution)/shard_map/ppermute | solution.py:26
  46.5 0.3 collective-permute-start.20
  46.8 0.2 collective-permute-done.10.b1
  46.9 3.6 %collective-permute-start.21 = (bf16[224,512]{1,0:T(8,128)(2,1)S(1)}, bf16[224,512]{1,0:T(8,128)(2,1)S(1)}, u32[]{:S(2)}, u32[]{:S(2)}) collective-permute-start(bf16[224,512]{1,0:T(8,128)(2,1)S(1)} %collective-permute-done.17.y2), channel_id=1, source_target_pairs={{0,1},{1,0},{2,3},{3,2},{4,5},{5,4},{6,7},{7,6},{8,9},{9,8},{10,11... | collective-permute-start | bytes 688136 | tf_op jit(solution)/shard_map/ppermute | solution.py:26
  50.6 3.3 %collective-permute-done.11.b2 = bf16[64,2176]{1,0:T(8,128)(2,1)S(1)} collective-permute-done((bf16[64,2176]{1,0:T(8,128)(2,1)S(1)}, bf16[64,2176]{1,0:T(8,128)(2,1)S(1)}, u32[]{:S(2)}, u32[]{:S(2)}) %collective-permute-start.11) | collective-permute-done | bytes 278560 | tf_op jit(solution)/shard_map/ppermute | solution.py:26
  53.9 2.5 %collective-permute-start.22 = (bf16[224,512]{1,0:T(8,128)(2,1)S(1)}, bf16[224,512]{1,0:T(8,128)(2,1)S(1)}, u32[]{:S(2)}, u32[]{:S(2)}) collective-permute-start(bf16[224,512]{1,0:T(8,128)(2,1)S(1)} %collective-permute-done.18.y3), channel_id=1, source_target_pairs={{0,1},{1,0},{2,3},{3,2},{4,5},{5,4},{6,7},{7,6},{8,9},{9,8},{10,11... | collective-permute-start | bytes 688136 | tf_op jit(solution)/shard_map/ppermute | solution.py:26
  56.4 1.7 %pack.1.w_all = bf16[1024,2048]{1,0:T(8,128)(2,1)S(1)} custom-call(bf16[2,64,2048]{2,1,0:T(8,128)(2,1)} %bitcast.25, bf16[2,64,2048]{2,1,0:T(8,128)(2,1)} %bitcast.27, bf16[32,2048]{1,0:T(8,128)(2,1)} %bitcast.33, bf16[32,2048]{1,0:T(8,128)(2,1)} %bitcast.35, bf16[64,2048]{1,0:T(8,128)(2,1)} %bitcast.29, bf16[64,2048]{1,0:T(8,128)(2,1)} %bitcast.31, ...), custom_call_target="tpu_custom_call" | custom-call | tf_op jit(solution)/shard_map/pack/pallas_call | solution.py:385
  58.1 1.9 %hidden.1 = (bf16[272,128]{1,0:T(8,128)(2,1)S(1)}, bf16[256,128]{1,0:T(8,128)(2,1)S(1)}) custom-call(bf16[64,2176]{1,0:T(8,128)(2,1)S(1)} %bitcast.20, bf16[64,2176]{1,0:T(8,128)(2,1)S(1)} %collective-permute-done.10.b1, bf16[64,2176]{1,0:T(8,128)(2,1)S(1)} %collective-permute-done.11.b2, bf16[64,2176]{1,0:T(8,128)(2,1)S(1)} %collective-permute-done.12.b3, ...), custom_call_target="tpu_custom_call" | custom-call | tf_op jit(solution)/shard_map/hidden/pallas_call | solution.py:408
  60.0 1.6 %collective-permute-start.13 = (bf16[272,128]{1,0:T(8,128)(2,1)S(1)}, bf16[272,128]{1,0:T(8,128)(2,1)S(1)}, u32[]{:S(2)}, u32[]{:S(2)}) collective-permute-start(bf16[272,128]{1,0:T(8,128)(2,1)S(1)} %get-tuple-element.59.h0), channel_id=1, source_target_pairs={{0,2},{2,4},{4,6},{6,0},{1,3},{3,5},{5,7},{7,1},{8,10},{10,12},{12... | collective-permute-start | bytes 208904 | tf_op jit(solution)/shard_map/ppermute | solution.py:26
  61.6 2.0 %collective-permute-start.14 = (bf16[272,128]{1,0:T(8,128)(2,1)S(1)}, bf16[272,128]{1,0:T(8,128)(2,1)S(1)}, u32[]{:S(2)}, u32[]{:S(2)}) collective-permute-start(bf16[272,128]{1,0:T(8,128)(2,1)S(1)} %get-tuple-element.59.h0), channel_id=1, source_target_pairs={{0,4},{2,6},{4,0},{6,2},{1,5},{3,7},{5,1},{7,3},{8,12},{10,14},{12... | collective-permute-start | bytes 208904 | tf_op jit(solution)/shard_map/ppermute | solution.py:26
  63.6 1.4 %collective-permute-start.15 = (bf16[272,128]{1,0:T(8,128)(2,1)S(1)}, bf16[272,128]{1,0:T(8,128)(2,1)S(1)}, u32[]{:S(2)}, u32[]{:S(2)}) collective-permute-start(bf16[272,128]{1,0:T(8,128)(2,1)S(1)} %get-tuple-element.59.h0), channel_id=1, source_target_pairs={{0,6},{2,0},{4,2},{6,4},{1,7},{3,1},{5,3},{7,5},{8,14},{10,8},{12,... | collective-permute-start | bytes 208904 | tf_op jit(solution)/shard_map/ppermute | solution.py:26
  65.0 0.1 arrange.1.d_all
  65.2 2.2 %collective-permute-done.14.h2 = bf16[272,128]{1,0:T(8,128)(2,1)S(1)} collective-permute-done((bf16[272,128]{1,0:T(8,128)(2,1)S(1)}, bf16[272,128]{1,0:T(8,128)(2,1)S(1)}, u32[]{:S(2)}, u32[]{:S(2)}) %collective-permute-start.14) | collective-permute-done | bytes 69664 | tf_op jit(solution)/shard_map/ppermute | solution.py:26
  67.3 0.7 down.1
  68.1 14.1 %all_to_all.15.back = bf16[32,8,512]{2,1,0:T(8,128)(2,1)S(1)} all-to-all(bf16[32,8,512]{2,1,0:T(8,128)(2,1)S(1)} %bitcast.21), channel_id=1, replica_groups=mesh['z'=8,'x'=4,'y'=4,'c'=2] {'z','x'}, dimensions={0} | all-to-all | bytes 524288 | tf_op jit(solution)/shard_map/all_to_all | solution.py:440
  82.2 0.7 sum.1
  82.9 6.8 %all-to-all-start.2 = ((f32[8,8,512]{2,1,0:T(8,128)}), f32[8,8,512]{2,1,0:T(8,128)S(1)}, u32[]{:S(2)}, u32[]{:S(2)}) async-start(f32[8,8,512]{2,1,0:T(8,128)} %sum.1), calls=%async_computation.2 | async-start | bytes 262144 | tf_op jit(solution)/shard_map/all_to_all | solution.py:449
  89.7 0.0 collective-permute-start.23
  89.7 2.6 %state.1 = f32[16,128,128]{2,1,0:T(8,128)} custom-call(f32[16,128]{1,0:T(8,128)S(1)} %get-tuple-element.68.keys, f32[16,128]{1,0:T(8,128)S(1)} %get-tuple-element.69.values, f32[16,128,128]{2,1,0:T(8,128)} %bitcast.23), custom_call_target="tpu_custom_call" | custom-call | tf_op jit(solution)/shard_map/state/pallas_call | solution.py:394
  92.3 2.6 %all-to-all-done.2.got = f32[8,8,512]{2,1,0:T(8,128)S(1)} async-done(((f32[8,8,512]{2,1,0:T(8,128)}), f32[8,8,512]{2,1,0:T(8,128)S(1)}, u32[]{:S(2)}, u32[]{:S(2)}) %all-to-all-start.2) | async-done | bytes 131104 | tf_op jit(solution)/shard_map/all_to_all | solution.py:449
  94.9 1.5 %last.1 = bf16[16,2048]{1,0:T(8,128)(2,1)} custom-call(f32[8,8,512]{2,1,0:T(8,128)S(1)} %all-to-all-done.2.got, bf16[8,2048]{1,0:T(8,128)(2,1)S(1)} %get-tuple-element.67.own, bf16[8,2048]{1,0:T(8,128)(2,1)S(1)} %collective-permute-done.23.other, f32[1,2048]{1,0:T(1,128)} %bitcast.37), custom_call_target="tpu_custom_call" | custom-call | tf_op jit(solution)/shard_map/last/pallas_call | solution.py:450
  (30 shorter events, 0.1 us)
Async XLA Ops:
  0.6 9.2 %copy-start = (bf16[2,2048,64]{1,2,0:T(8,128)(2,1)S(1)}, bf16[2,2048,64]{1,2,0:T(8,128)(2,1)}, u32[]{:S(2)}) copy-start(bf16[2,2048,64]{1,2,0:T(8,128)(2,1)} %param.36) | copy-start | bytes 1572868
  0.6 9.6 %copy-start.1 = (bf16[2,2048,64]{1,2,0:T(8,128)(2,1)S(1)}, bf16[2,2048,64]{1,2,0:T(8,128)(2,1)}, u32[]{:S(2)}) copy-start(bf16[2,2048,64]{1,2,0:T(8,128)(2,1)} %param.37) | copy-start | bytes 1572868
  0.7 13.8 %copy-start.4 = (bf16[2048,32]{0,1:T(8,128)(2,1)S(1)}, bf16[2048,32]{0,1:T(8,128)(2,1)}, u32[]{:S(2)}) copy-start(bf16[2048,32]{0,1:T(8,128)(2,1)} %param.43) | copy-start | bytes 393220
  0.7 16.8 %copy-start.5 = (bf16[2048,32]{0,1:T(8,128)(2,1)S(1)}, bf16[2048,32]{0,1:T(8,128)(2,1)}, u32[]{:S(2)}) copy-start(bf16[2048,32]{0,1:T(8,128)(2,1)} %param.44) | copy-start | bytes 393220
  0.7 15.7 %copy-start.2 = (bf16[2048,64]{0,1:T(8,128)(2,1)S(1)}, bf16[2048,64]{0,1:T(8,128)(2,1)}, u32[]{:S(2)}) copy-start(bf16[2048,64]{0,1:T(8,128)(2,1)} %param.39) | copy-start | bytes 786436
  0.7 15.8 %copy-start.3 = (bf16[2048,64]{0,1:T(8,128)(2,1)S(1)}, bf16[2048,64]{0,1:T(8,128)(2,1)}, u32[]{:S(2)}) copy-start(bf16[2048,64]{0,1:T(8,128)(2,1)} %param.40) | copy-start | bytes 786436
  0.7 9.1 %copy-start.6 = (bf16[2048]{0:T(1024)(128)(2,1)S(1)}, bf16[2048]{0:T(1024)(128)(2,1)}, u32[]{:S(2)}) copy-start(bf16[2048]{0:T(1024)(128)(2,1)} %param.42) | copy-start | bytes 12292
  5.7 4.1 %collective-permute-start = (bf16[8,2048]{1,0:T(8,128)(2,1)S(1)}, bf16[8,2048]{1,0:T(8,128)(2,1)S(1)}, u32[]{:S(2)}, u32[]{:S(2)}) collective-permute-start(bf16[8,2048]{1,0:T(8,128)(2,1)S(1)} %get-tuple-element.37), channel_id=1, source_target_pairs={{0,1},{1,0},{2,3},{3,2},{4,5},{5,4},{6,7},{7,6},{8,9},{9,8},{10,11... | collective-permute-start | bytes 98312 | tf_op jit(solution)/shard_map/ppermute | solution.py:26
  9.8 9.7 %collective-permute-start.1 = (bf16[2,64,2048]{2,1,0:T(8,128)(2,1)S(1)}, bf16[2,64,2048]{2,1,0:T(8,128)(2,1)S(1)}, u32[]{:S(2)}, u32[]{:S(2)}) collective-permute-start(bf16[2,64,2048]{2,1,0:T(8,128)(2,1)S(1)} %bitcast.26), channel_id=1, source_target_pairs={{0,1},{1,0},{2,3},{3,2},{4,5},{5,4},{6,7},{7,6},{8,9},{9,8},{10,11... | collective-permute-start | bytes 1572872 | tf_op jit(solution)/shard_map/ppermute | solution.py:26
  10.3 9.2 %collective-permute-start.2 = (bf16[2,64,2048]{2,1,0:T(8,128)(2,1)S(1)}, bf16[2,64,2048]{2,1,0:T(8,128)(2,1)S(1)}, u32[]{:S(2)}, u32[]{:S(2)}) collective-permute-start(bf16[2,64,2048]{2,1,0:T(8,128)(2,1)S(1)} %bitcast.28), channel_id=1, source_target_pairs={{0,1},{1,0},{2,3},{3,2},{4,5},{5,4},{6,7},{7,6},{8,9},{9,8},{10,11... | collective-permute-start | bytes 1572872 | tf_op jit(solution)/shard_map/ppermute | solution.py:26
  10.4 4.0 %collective-permute-start.7 = (bf16[8,2048]{1,0:T(8,128)(2,1)S(1)}, bf16[8,2048]{1,0:T(8,128)(2,1)S(1)}, u32[]{:S(2)}, u32[]{:S(2)}) collective-permute-start(bf16[8,2048]{1,0:T(8,128)(2,1)S(1)} %add_convert_fusion.pair), channel_id=1, source_target_pairs={{0,2},{2,4},{4,6},{6,0},{1,3},{3,5},{5,7},{7,1},{8,10},{10,12},{12... | collective-permute-start | bytes 98312 | tf_op jit(solution)/shard_map/ppermute | solution.py:26
  10.5 5.9 %collective-permute-start.8 = (bf16[8,2048]{1,0:T(8,128)(2,1)S(1)}, bf16[8,2048]{1,0:T(8,128)(2,1)S(1)}, u32[]{:S(2)}, u32[]{:S(2)}) collective-permute-start(bf16[8,2048]{1,0:T(8,128)(2,1)S(1)} %add_convert_fusion.pair), channel_id=1, source_target_pairs={{0,4},{2,6},{4,0},{6,2},{1,5},{3,7},{5,1},{7,3},{8,12},{10,14},{12... | collective-permute-start | bytes 98312 | tf_op jit(solution)/shard_map/ppermute | solution.py:26
  12.7 3.8 %collective-permute-start.9 = (bf16[8,2048]{1,0:T(8,128)(2,1)S(1)}, bf16[8,2048]{1,0:T(8,128)(2,1)S(1)}, u32[]{:S(2)}, u32[]{:S(2)}) collective-permute-start(bf16[8,2048]{1,0:T(8,128)(2,1)S(1)} %add_convert_fusion.pair), channel_id=1, source_target_pairs={{0,6},{2,0},{4,2},{6,4},{1,7},{3,1},{5,3},{7,5},{8,14},{10,8},{12,... | collective-permute-start | bytes 98312 | tf_op jit(solution)/shard_map/ppermute | solution.py:26
  14.4 3.1 %collective-permute-start.3 = (bf16[32,2048]{1,0:T(8,128)(2,1)S(1)}, bf16[32,2048]{1,0:T(8,128)(2,1)S(1)}, u32[]{:S(2)}, u32[]{:S(2)}) collective-permute-start(bf16[32,2048]{1,0:T(8,128)(2,1)S(1)} %bitcast.34), channel_id=1, source_target_pairs={{0,1},{1,0},{2,3},{3,2},{4,5},{5,4},{6,7},{7,6},{8,9},{9,8},{10,11... | collective-permute-start | bytes 393224 | tf_op jit(solution)/shard_map/ppermute | solution.py:26
  16.4 3.2 %collective-permute-start.5 = (bf16[64,2048]{1,0:T(8,128)(2,1)S(1)}, bf16[64,2048]{1,0:T(8,128)(2,1)S(1)}, u32[]{:S(2)}, u32[]{:S(2)}) collective-permute-start(bf16[64,2048]{1,0:T(8,128)(2,1)S(1)} %bitcast.30), channel_id=1, source_target_pairs={{0,1},{1,0},{2,3},{3,2},{4,5},{5,4},{6,7},{7,6},{8,9},{9,8},{10,11... | collective-permute-start | bytes 786440 | tf_op jit(solution)/shard_map/ppermute | solution.py:26
  16.5 3.1 %collective-permute-start.6 = (bf16[64,2048]{1,0:T(8,128)(2,1)S(1)}, bf16[64,2048]{1,0:T(8,128)(2,1)S(1)}, u32[]{:S(2)}, u32[]{:S(2)}) collective-permute-start(bf16[64,2048]{1,0:T(8,128)(2,1)S(1)} %bitcast.32), channel_id=1, source_target_pairs={{0,1},{1,0},{2,3},{3,2},{4,5},{5,4},{6,7},{7,6},{8,9},{9,8},{10,11... | collective-permute-start | bytes 786440 | tf_op jit(solution)/shard_map/ppermute | solution.py:26
  17.5 2.0 %collective-permute-start.4 = (bf16[32,2048]{1,0:T(8,128)(2,1)S(1)}, bf16[32,2048]{1,0:T(8,128)(2,1)S(1)}, u32[]{:S(2)}, u32[]{:S(2)}) collective-permute-start(bf16[32,2048]{1,0:T(8,128)(2,1)S(1)} %bitcast.36), channel_id=1, source_target_pairs={{0,1},{1,0},{2,3},{3,2},{4,5},{5,4},{6,7},{7,6},{8,9},{9,8},{10,11... | collective-permute-start | bytes 393224 | tf_op jit(solution)/shard_map/ppermute | solution.py:26
  19.5 19.6 %all-to-all-start = ((bf16[8,8,2176]{2,1,0:T(8,128)(2,1)}), bf16[8,8,2176]{2,1,0:T(8,128)(2,1)S(1)}, u32[]{:S(2)}, u32[]{:S(2)}) async-start(bf16[8,8,2176]{2,1,0:T(8,128)(2,1)} %get-tuple-element.51), calls=%async_computation | async-start | bytes 557056 | tf_op jit(solution)/shard_map/all_to_all | solution.py:380
  27.6 15.2 %collective-permute-start.16 = (bf16[224,512]{1,0:T(8,128)(2,1)}, bf16[224,512]{1,0:T(8,128)(2,1)S(1)}, u32[]{:S(2)}, u32[]{:S(2)}) collective-permute-start(bf16[224,512]{1,0:T(8,128)(2,1)} %get-tuple-element.62), channel_id=1, source_target_pairs={{0,2},{2,4},{4,6},{6,0},{1,3},{3,5},{5,7},{7,1},{8,10},{10,12},{12... | collective-permute-start | bytes 688136 | tf_op jit(solution)/shard_map/ppermute | solution.py:26
  27.9 16.0 %collective-permute-start.17 = (bf16[224,512]{1,0:T(8,128)(2,1)}, bf16[224,512]{1,0:T(8,128)(2,1)S(1)}, u32[]{:S(2)}, u32[]{:S(2)}) collective-permute-start(bf16[224,512]{1,0:T(8,128)(2,1)} %get-tuple-element.63), channel_id=1, source_target_pairs={{0,4},{2,6},{4,0},{6,2},{1,5},{3,7},{5,1},{7,3},{8,12},{10,14},{12... | collective-permute-start | bytes 688136 | tf_op jit(solution)/shard_map/ppermute | solution.py:26
  31.1 15.4 %collective-permute-start.18 = (bf16[224,512]{1,0:T(8,128)(2,1)S(1)}, bf16[224,512]{1,0:T(8,128)(2,1)S(1)}, u32[]{:S(2)}, u32[]{:S(2)}) collective-permute-start(bf16[224,512]{1,0:T(8,128)(2,1)S(1)} %get-tuple-element.64), channel_id=1, source_target_pairs={{0,6},{2,0},{4,2},{6,4},{1,7},{3,1},{5,3},{7,5},{8,14},{10,8},{12,... | collective-permute-start | bytes 688136 | tf_op jit(solution)/shard_map/ppermute | solution.py:26
  39.2 7.8 %collective-permute-start.10 = (bf16[64,2176]{1,0:T(8,128)(2,1)S(1)}, bf16[64,2176]{1,0:T(8,128)(2,1)S(1)}, u32[]{:S(2)}, u32[]{:S(2)}) collective-permute-start(bf16[64,2176]{1,0:T(8,128)(2,1)S(1)} %bitcast.17), channel_id=1, source_target_pairs={{0,8},{8,16},{16,24},{24,0},{1,9},{9,17},{17,25},{25,1},{2,10},{10... | collective-permute-start | bytes 835592 | tf_op jit(solution)/shard_map/ppermute | solution.py:26
  40.4 13.5 %collective-permute-start.11 = (bf16[64,2176]{1,0:T(8,128)(2,1)S(1)}, bf16[64,2176]{1,0:T(8,128)(2,1)S(1)}, u32[]{:S(2)}, u32[]{:S(2)}) collective-permute-start(bf16[64,2176]{1,0:T(8,128)(2,1)S(1)} %bitcast.18), channel_id=1, source_target_pairs={{0,16},{8,24},{16,0},{24,8},{1,17},{9,25},{17,1},{25,9},{2,18},{10... | collective-permute-start | bytes 835592 | tf_op jit(solution)/shard_map/ppermute | solution.py:26
  42.8 15.3 %collective-permute-start.12 = (bf16[64,2176]{1,0:T(8,128)(2,1)S(1)}, bf16[64,2176]{1,0:T(8,128)(2,1)S(1)}, u32[]{:S(2)}, u32[]{:S(2)}) collective-permute-start(bf16[64,2176]{1,0:T(8,128)(2,1)S(1)} %bitcast.19), channel_id=1, source_target_pairs={{0,24},{8,0},{16,8},{24,16},{1,25},{9,1},{17,9},{25,17},{2,26},{10... | collective-permute-start | bytes 835592 | tf_op jit(solution)/shard_map/ppermute | solution.py:26
  44.0 17.6 %collective-permute-start.19 = (bf16[224,512]{1,0:T(8,128)(2,1)S(1)}, bf16[224,512]{1,0:T(8,128)(2,1)S(1)}, u32[]{:S(2)}, u32[]{:S(2)}) collective-permute-start(bf16[224,512]{1,0:T(8,128)(2,1)S(1)} %get-tuple-element.61.y0), channel_id=1, source_target_pairs={{0,1},{1,0},{2,3},{3,2},{4,5},{5,4},{6,7},{7,6},{8,9},{9,8},{10,11... | collective-permute-start | bytes 688136 | tf_op jit(solution)/shard_map/ppermute | solution.py:26
  46.5 17.1 %collective-permute-start.20 = (bf16[224,512]{1,0:T(8,128)(2,1)S(1)}, bf16[224,512]{1,0:T(8,128)(2,1)S(1)}, u32[]{:S(2)}, u32[]{:S(2)}) collective-permute-start(bf16[224,512]{1,0:T(8,128)(2,1)S(1)} %collective-permute-done.16.y1), channel_id=1, source_target_pairs={{0,1},{1,0},{2,3},{3,2},{4,5},{5,4},{6,7},{7,6},{8,9},{9,8},{10,11... | collective-permute-start | bytes 688136 | tf_op jit(solution)/shard_map/ppermute | solution.py:26
  46.9 18.1 %collective-permute-start.21 = (bf16[224,512]{1,0:T(8,128)(2,1)S(1)}, bf16[224,512]{1,0:T(8,128)(2,1)S(1)}, u32[]{:S(2)}, u32[]{:S(2)}) collective-permute-start(bf16[224,512]{1,0:T(8,128)(2,1)S(1)} %collective-permute-done.17.y2), channel_id=1, source_target_pairs={{0,1},{1,0},{2,3},{3,2},{4,5},{5,4},{6,7},{7,6},{8,9},{9,8},{10,11... | collective-permute-start | bytes 688136 | tf_op jit(solution)/shard_map/ppermute | solution.py:26
  53.9 11.1 %collective-permute-start.22 = (bf16[224,512]{1,0:T(8,128)(2,1)S(1)}, bf16[224,512]{1,0:T(8,128)(2,1)S(1)}, u32[]{:S(2)}, u32[]{:S(2)}) collective-permute-start(bf16[224,512]{1,0:T(8,128)(2,1)S(1)} %collective-permute-done.18.y3), channel_id=1, source_target_pairs={{0,1},{1,0},{2,3},{3,2},{4,5},{5,4},{6,7},{7,6},{8,9},{9,8},{10,11... | collective-permute-start | bytes 688136 | tf_op jit(solution)/shard_map/ppermute | solution.py:26
  60.0 5.1 %collective-permute-start.13 = (bf16[272,128]{1,0:T(8,128)(2,1)S(1)}, bf16[272,128]{1,0:T(8,128)(2,1)S(1)}, u32[]{:S(2)}, u32[]{:S(2)}) collective-permute-start(bf16[272,128]{1,0:T(8,128)(2,1)S(1)} %get-tuple-element.59.h0), channel_id=1, source_target_pairs={{0,2},{2,4},{4,6},{6,0},{1,3},{3,5},{5,7},{7,1},{8,10},{10,12},{12... | collective-permute-start | bytes 208904 | tf_op jit(solution)/shard_map/ppermute | solution.py:26
  61.6 5.7 %collective-permute-start.14 = (bf16[272,128]{1,0:T(8,128)(2,1)S(1)}, bf16[272,128]{1,0:T(8,128)(2,1)S(1)}, u32[]{:S(2)}, u32[]{:S(2)}) collective-permute-start(bf16[272,128]{1,0:T(8,128)(2,1)S(1)} %get-tuple-element.59.h0), channel_id=1, source_target_pairs={{0,4},{2,6},{4,0},{6,2},{1,5},{3,7},{5,1},{7,3},{8,12},{10,14},{12... | collective-permute-start | bytes 208904 | tf_op jit(solution)/shard_map/ppermute | solution.py:26
  63.6 3.8 %collective-permute-start.15 = (bf16[272,128]{1,0:T(8,128)(2,1)S(1)}, bf16[272,128]{1,0:T(8,128)(2,1)S(1)}, u32[]{:S(2)}, u32[]{:S(2)}) collective-permute-start(bf16[272,128]{1,0:T(8,128)(2,1)S(1)} %get-tuple-element.59.h0), channel_id=1, source_target_pairs={{0,6},{2,0},{4,2},{6,4},{1,7},{3,1},{5,3},{7,5},{8,14},{10,8},{12,... | collective-permute-start | bytes 208904 | tf_op jit(solution)/shard_map/ppermute | solution.py:26
  82.9 12.0 %all-to-all-start.2 = ((f32[8,8,512]{2,1,0:T(8,128)}), f32[8,8,512]{2,1,0:T(8,128)S(1)}, u32[]{:S(2)}, u32[]{:S(2)}) async-start(f32[8,8,512]{2,1,0:T(8,128)} %sum.1), calls=%async_computation.2 | async-start | bytes 262144 | tf_op jit(solution)/shard_map/all_to_all | solution.py:449
  89.7 2.6 %collective-permute-start.23 = (bf16[8,2048]{1,0:T(8,128)(2,1)S(1)}, bf16[8,2048]{1,0:T(8,128)(2,1)S(1)}, u32[]{:S(2)}, u32[]{:S(2)}) collective-permute-start(bf16[8,2048]{1,0:T(8,128)(2,1)S(1)} %get-tuple-element.67.own), channel_id=1, source_target_pairs={{0,1},{1,0},{2,3},{3,2},{4,5},{5,4},{6,7},{7,6},{8,9},{9,8},{10,11... | collective-permute-start | bytes 98312 | tf_op jit(solution)/shard_map/ppermute | solution.py:26
where the time goes:
time: 97 us; the launch traced here: 96.5 us
  starting transfers between devices  47.7 us (49%)
  waiting for transfers between devices  17.7 us (18%)
  Pallas kernels  16 us (16%)
  blocking collectives  14.1 us (15%)
    ppermute x24, starting transfers between devices, shifted(): return lax.ppermute(value, axis, [(i, (i + step) % n) for i in range(n)])  32.8 us
    all_to_all x1, blocking collectives, layer(): back = lax.all_to_all(partial.reshape(32, 8, 512), EP, 0, 0, tiled=True)  14.1 us
    all_to_all x1, starting transfers between devices, layer(): block = lax.all_to_all(sent, 'z', 0, 0, tiled=True).reshape(64, 2176)  8.09 us
    all_to_all x1, waiting for transfers between devices, layer(): block = lax.all_to_all(sent, 'z', 0, 0, tiled=True).reshape(64, 2176)  7.81 us
    ppermute x24, waiting for transfers between devices, shifted(): return lax.ppermute(value, axis, [(i, (i + step) % n) for i in range(n)])  7.26 us
    all_to_all x1, starting transfers between devices, layer(): got = lax.all_to_all(mine, TP, 0, 0, tiled=True)  6.79 us
    pallas_call x1, Pallas kernels, layer(): pl.pallas_call(mixer_kernel, in_specs=[SM, VM, VM, VM] + [HB] * 9, out_sp...  4.93 us
    all_to_all x1, waiting for transfers between devices, layer(): got = lax.all_to_all(mine, TP, 0, 0, tiled=True)  2.65 us
  transfers between devices with their start and end apart: 26, of which 7 were waited for; matrix products, arithmetic and copies ran while one was open for 0% of the time, Pallas kernels for 8%

commit v1 on v0

--- a/solution.py
+++ b/solution.py
@@ -56,18 +56,22 @@
 
 
 def mixer_kernel(
-    lengths, frequency, tokens, gain, wq, wk, wv, wg, state, ow, ed, dd, sd,
-    kept, given, key_out, value_out, d0, d1, d2, d3,
-    bq, bk, bv, bg, bs, bo, rows, sems, dsems,
+    lengths, frequency, tokens, gain, wq, wk, wv, wg, state, ow, ed, dd, sd, ids, ews, gain1, gain2,
+    kept, given, key_out, value_out, d0, d1, d2, d3, mine, info, g1, g2,
+    bl, bf, bt, bn, bq, bk, bv, bg, bs, bo, bi, bw, rows, table, sems, dsems,
 ):
     moves = [
         pltpu.make_async_copy(src, dst, sems.at[i])
         for i, (src, dst) in enumerate(
-            ((wq, bq), (wk, bk), (state, bs), (wv, bv), (wg, bg), (ow, bo))
+            (
+                (wq, bq), (wk, bk), (state, bs), (wv, bv), (wg, bg), (ow, bo),
+                (lengths, bl), (frequency, bf), (tokens, bt), (gain, bn),
+                (ids, bi), (ews, bw), (gain1, g1), (gain2, g2),
+            )
         )
     ]
-    for move in moves:
-        move.start()
+    for i in (6, 7, 8, 0, 1, 2, 3, 4, 5, 9, 10, 11, 12, 13):
+        moves[i].start()
     slices = []
     for k, out in enumerate((d0, d1, d2, d3)):
         cols = pl.ds(pl.multiple_of(lax.rem(lax.axis_index("y") + k, 4) * 512, 512), 512)
@@ -80,15 +84,21 @@
             c = pltpu.make_async_copy(src, dst, dsems.at[len(slices)])
             c.start()
             slices.append(c)
-    f = frequency[...]
+    first = lax.axis_index("c") == 0
+    moves[6].wait()
+    moves[7].wait()
+    f = bf[...]
     for i in range(16):
-        rows[i : i + 1, :] = jnp.full((1, 128), lengths[i].astype(F32), F32) * f
+        rows[i : i + 1, :] = jnp.full((1, 128), bl[i].astype(F32), F32) * f
     angles = rows[...]
     lane = lax.broadcasted_iota(jnp.int32, (16, 128), 1)
     cos2 = jnp.cos(angles)
     sin2 = jnp.sin(angles) * jnp.where(lane < 64, -1.0, 1.0)
     decay = decay_row()
-    t = tokens[...]
+    moves[8].wait()
+    t = bt[...]
+    wide = t.astype(F32)
+    mine[...] = jnp.where(first, wide[:8], wide[8:]).astype(BF)
 
     def turned(v):
         return v * cos2 + pltpu.roll(v, 64, 1) * sin2
@@ -109,14 +119,24 @@
     g = dot(t, bg[...])
     match = jnp.sum(q * k, axis=1, keepdims=True)
     readout = decay * rows[...] + match * v
-    mixed = (norm(readout, gain[...]) * silu(g)).astype(BF)
+    moves[9].wait()
+    mixed = (norm(readout, bn[...]) * silu(g)).astype(BF)
     moves[5].wait()
     partial = dot(mixed, bo[...])
     low, high = partial[:8], partial[8:]
-    first = lax.axis_index("c") == 0
     kept[...] = jnp.where(first, low, high).astype(BF)
     given[...] = jnp.where(first, high, low).astype(BF)
-    for c in slices:
+    moves[10].wait()
+    moves[11].wait()
+    table[...] = jnp.zeros((128, 128), F32)
+    w = bw[...]
+    top = w.astype(BF).astype(F32)
+    table[0:6, 0:16] = bi[...].astype(F32)
+    table[8:14, 0:16] = top
+    table[16:22, 0:16] = w - top
+    f = table[...].T
+    info[...] = jnp.where(first, f[0:8], f[8:16]).astype(BF)
+    for c in (moves[12], moves[13], *slices):
         c.wait()
 
 
@@ -164,32 +184,27 @@
     store.wait()
 
 
-def after_kernel(pair, r1, r2, r3, tokens, gain, ids, ews, after, sent, table):
-    first = lax.axis_index("c") == 0
-    table[...] = jnp.zeros((128, 128), F32)
-    w = ews[...]
-    high = w.astype(BF).astype(F32)
-    table[0:6, 0:16] = ids[...].astype(F32)
-    table[8:14, 0:16] = high
-    table[16:22, 0:16] = w - high
-    f = table[...].T
-    f = jnp.where(first, f[0:8], f[8:16]).astype(BF)
-    t = tokens[...].astype(F32)
-    mine = jnp.where(first, t[:8], t[8:])
+def after_kernel(pair, r1, r2, r3, mine, gain, info, after, sent):
     branch = pair[...].astype(F32)
     for r in (r1, r2, r3):
         branch = branch + r[...].astype(F32)
-    a = norm(RESIDUAL_SCALE * mine + branch, gain[...]).astype(BF)
+    a = norm(RESIDUAL_SCALE * mine[...].astype(F32) + branch, gain[...]).astype(BF)
     after[...] = a
+    f = info[...]
     for j in range(8):
         sent[j, :, 0:2048] = a
         sent[j, :, 2048:2176] = f
 
 
-def hidden_kernel(b0, b1, b2, b3, w_all, side, h_out, pt_out, acts, info, xo, xp):
-    for k, b in enumerate((b0, b1, b2, b3)):
+def hidden_kernel(b0, b1, b3, near_half, far_half, w_all, side, h_out, pt_out, acts, info, xo, xp):
+    for k, b in ((0, b0), (1, b1), (3, b3)):
         acts[64 * k : 64 * k + 64, :] = b[:, 0:2048]
         info[64 * k : 64 * k + 64, :] = b[:, 2048:2176].astype(F32)
+    odd = lax.rem(lax.axis_index("y"), 2) * 32
+    for start, b in ((128 + odd, near_half), (160 - odd, far_half)):
+        here = pl.ds(pl.multiple_of(start, 32), 32)
+        acts[here, :] = b[:, 0:2048]
+        info[here, :] = b[:, 2048:2176].astype(F32)
     a = acts[...]
     lane = lax.broadcasted_iota(jnp.int32, (256, 128), 1)
     row = lax.broadcasted_iota(jnp.int32, (256, 128), 0)
@@ -274,20 +289,22 @@
     total = shared[...]
     for j in range(32):
         total = total + back[j].astype(F32)
-    for j in range(8):
-        out[j] = total
-
-
-def last_kernel(got, own, other, gain, out):
+    out[...] = total
+
+
+def last_kernel(s0, s1, s2, s3, after, gain, out, whole):
+    for k, s in enumerate((s0, s1, s2, s3)):
+        start = lax.rem(lax.axis_index("y") + 4 - k, 4) * 512
+        whole[:, pl.ds(pl.multiple_of(start, 512), 512)] = s[...]
+    out[...] = norm(RESIDUAL_SCALE * after[...].astype(F32) + whole[...], gain[...]).astype(BF)
+
+
+def join_kernel(own, other, out):
     first = lax.axis_index("c") == 0
-    mine, theirs = own[...].astype(F32), other[...].astype(F32)
-    low = jnp.where(first, mine, theirs)
-    high = jnp.where(first, theirs, mine)
-    rows = []
-    for c, residual in enumerate((low, high)):
-        side = jnp.concatenate([got[2 * y + c] for y in range(4)], axis=1)
-        rows.append(norm(RESIDUAL_SCALE * residual + side, gain[...]))
-    out[...] = jnp.concatenate(rows, axis=0).astype(BF)
+    a, b = own[...].astype(F32), other[...].astype(F32)
+    low = jnp.where(first, a, b)
+    high = jnp.where(first, b, a)
+    out[...] = jnp.concatenate([low, high], axis=0).astype(BF)
 
 
 def limit(mib):
@@ -333,26 +350,47 @@
 ):
     frequency = np.asarray(1.0 / 10000.0 ** ((np.arange(128) % 64) / 64.0), np.float32)
     state = old_state.reshape(16, 128, 128)
-    kept, given, keys, values, *downs = pl.pallas_call(
+    outs = pl.pallas_call(
         mixer_kernel,
-        in_specs=[SM, VM, VM, VM] + [HB] * 9,
-        out_specs=[VM] * 8,
-        out_shape=[shape(8, 2048)] * 2 + [shape(16, 128, dtype=F32)] * 2 + [shape(224, 512)] * 4,
-        scratch_shapes=[pltpu.VMEM((2048, 128), BF)] * 4
+        in_specs=[HB] * 17,
+        out_specs=[VM] * 12,
+        out_shape=[shape(8, 2048)] * 2
+        + [shape(16, 128, dtype=F32)] * 2
+        + [shape(224, 512)] * 4
+        + [shape(8, 2048), shape(8, 128)]
+        + [shape(1, 2048, dtype=F32)] * 2,
+        scratch_shapes=[
+            pltpu.SMEM((16,), jnp.int32),
+            pltpu.VMEM((1, 128), F32),
+            pltpu.VMEM((16, 2048), BF),
+            pltpu.VMEM((1, 128), F32),
+        ]
+        + [pltpu.VMEM((2048, 128), BF)] * 4
         + [
             pltpu.VMEM((16, 128, 128), F32),
             pltpu.VMEM((128, 2048), BF),
+            pltpu.VMEM((6, 16), jnp.int32),
+            pltpu.VMEM((6, 16), F32),
             pltpu.VMEM((16, 128), F32),
-            pltpu.SemaphoreType.DMA((6,)),
+            pltpu.VMEM((128, 128), F32),
+            pltpu.SemaphoreType.DMA((14,)),
             pltpu.SemaphoreType.DMA((16,)),
         ],
         compiler_params=limit(8),
         name="mixer",
     )(
-        big(lengths), big(jnp.asarray(frequency)[None]), big(tokens), big(head_gain.reshape(1, 128)),
-        big(query_weight), big(key_weight), big(value_weight), big(gate_weight), big(state),
-        big(output_weight), big(expert_down), big(dense_down), big(shared_down),
+        *[
+            big(v)
+            for v in (
+                lengths, jnp.asarray(frequency)[None], tokens, head_gain.reshape(1, 128),
+                query_weight, key_weight, value_weight, gate_weight, state, output_weight,
+                expert_down, dense_down, shared_down, expert_ids.T, expert_weights.T,
+                first_gain.reshape(1, 2048), second_gain.reshape(1, 2048),
+            )
+        ]
     )
+    kept, given, keys, values = outs[0:4]
+    downs, (mine, info, g1, g2) = outs[4:8], outs[8:12]
 
     pair = (kept.astype(F32) + shifted(given, "c", 1).astype(F32)).astype(BF)
     raw = (
@@ -360,27 +398,25 @@
         dense_gate.T, dense_up.T, shared_gate.T, shared_up.T,
     )
     side = jnp.broadcast_to(side_gate[None], (8, 2048))
-    raw, side, pair = lax.optimization_barrier((raw, side, pair))
+    side, downs, pair = lax.optimization_barrier((side, downs, pair))
     arrived = [shifted(pair, "y", k) for k in range(1, 4)]
-    peers = [shifted(r, "c", 1) for r in raw]
+    from_y = [downs[0]] + [shifted(downs[k], "y", k) for k in range(1, 4)]
     after, sent = pl.pallas_call(
         after_kernel,
-        in_specs=[VM] * 8,
+        in_specs=[VM] * 7,
         out_specs=[VM, VM],
         out_shape=[shape(8, 2048), jax.ShapeDtypeStruct((8, 8, 2176), BF)],
-        scratch_shapes=[pltpu.VMEM((128, 128), F32)],
         compiler_params=limit(4),
         name="after",
-    )(
-        pair, *arrived, big(tokens), big(first_gain.reshape(1, 2048)),
-        big(expert_ids.T), big(expert_weights.T),
-    )
-
-    peers, downs, side, sent = lax.optimization_barrier((peers, downs, side, sent))
+    )(pair, *arrived, mine, g1, info)
+
+    raw, side, sent = lax.optimization_barrier((raw, side, sent))
+    peers = [shifted(r, "c", 1) for r in raw]
     block = lax.all_to_all(sent, "z", 0, 0, tiled=True).reshape(64, 2176)
-    from_y = [downs[0]] + [shifted(downs[k], "y", k) for k in range(1, 4)]
-    blocks = [block] + [shifted(block, "x", k) for k in range(1, 4)]
-    other = shifted(after, "c", 1)
+    part = lax.dynamic_slice_in_dim(block, (lax.axis_index("y") % 2) * 32, 32, 0)
+    near_half = shifted(part, "x", 2)
+    far_half = lax.ppermute(near_half, "y", [(0, 1), (1, 0), (2, 3), (3, 2)])
+    blocks = [block] + [shifted(block, "x", k) for k in (1, 3)] + [near_half, far_half]
     from_c = [shifted(d, "c", 1) for d in from_y]
     w_all = pl.pallas_call(
         pack_kernel,
@@ -407,7 +443,7 @@
 
     hidden, slots = pl.pallas_call(
         hidden_kernel,
-        in_specs=[VM] * 6,
+        in_specs=[VM] * 7,
         out_specs=[VM] * 2,
         out_shape=[shape(272, 128), shape(256, 128)],
         scratch_shapes=[
@@ -438,23 +474,32 @@
     )(*gathered, slots, near(d_all))
 
     back = lax.all_to_all(partial.reshape(32, 8, 512), EP, 0, 0, tiled=True)
-    mine = pl.pallas_call(
+    total = pl.pallas_call(
         sum_kernel,
         in_specs=[VM, VM],
         out_specs=VM,
-        out_shape=jax.ShapeDtypeStruct((8, 8, 512), F32),
+        out_shape=shape(8, 512, dtype=F32),
         compiler_params=limit(3),
         name="sum",
     )(back, shared)
-    got = lax.all_to_all(mine, TP, 0, 0, tiled=True)
+    pieces = [total] + [shifted(total, "y", k) for k in range(1, 4)]
+    final = pl.pallas_call(
+        last_kernel,
+        in_specs=[VM] * 6,
+        out_specs=VM,
+        out_shape=shape(8, 2048),
+        scratch_shapes=[pltpu.VMEM((8, 2048), F32)],
+        compiler_params=limit(3),
+        name="last",
+    )(*pieces, after, g2)
     layer_out = pl.pallas_call(
-        last_kernel,
-        in_specs=[VM] * 4,
+        join_kernel,
+        in_specs=[VM] * 2,
         out_specs=VM,
         out_shape=jax.ShapeDtypeStruct((16, 2048), BF),
         compiler_params=limit(3),
-        name="last",
-    )(got, after, other, big(second_gain.reshape(1, 2048)))
+        name="join",
+    )(final, shifted(final, "c", 1))
     return (layer_out, new_state.reshape(16, 1, 128, 128))
 
 

time: 97 us -> 103 us (1.062)
  waiting for transfers between devices: 17.7 us -> 26.5 us
  blocking collectives: 14.1 us -> 18.7 us
  Pallas kernels: 16 us -> 12.3 us
  starting transfers between devices: 47.7 us -> 44.1 us
    ppermute x24 -> x27, waiting for transfers between devices: 7.26 us -> 23.8 us  [shifted(): return lax.ppermute(value, axis, [(i, (i + step) % n) for i in range(n)])]
    all_to_all x1, waiting for transfers between devices: 7.81 us -> 0.01 us  [layer(): block = lax.all_to_all(sent, 'z', 0, 0, tiled=True).reshape(64, 2176)]
    all_to_all x1 -> x0, starting transfers between devices: 6.79 us -> none  [layer(): got = lax.all_to_all(mine, TP, 0, 0, tiled=True)]
    all_to_all x1, blocking collectives: 14.1 us -> 18.7 us  [layer(): back = lax.all_to_all(partial.reshape(32, 8, 512), EP, 0, 0, tiled=True)]
    pallas_call x5 -> x6, Pallas kernels: 10.9 us -> 7.19 us  [the longest x1 3.43 us: layer(): pl.pallas_call(mixer_kernel, in_specs=[HB] * 17, out_specs=[VM] * 12, out...]
    ppermute x0 -> x1, waiting for transfers between devices: none -> 2.69 us  [layer(): far_half = lax.ppermute(near_half, 'y', [(0, 1), (1, 0), (2, 3), (3, 2)])]
    all_to_all x1 -> x0, waiting for transfers between devices: 2.65 us -> none  [layer(): got = lax.all_to_all(mine, TP, 0, 0, tiled=True)]
    ppermute x24 -> x27, starting transfers between devices: 32.8 us -> 35.5 us  [shifted(): return lax.ppermute(value, axis, [(i, (i + step) % n) for i in range(n)])]
  transfers between devices with their start and end apart: 26 -> 29, of which waited for: 7 -> 13; matrix products, arithmetic and copies ran while one was open for 0% -> 0% of each run, Pallas kernels for 8% -> 6%
where the time goes in v1:
time: 103 us; the launch traced here: 102 us
  starting transfers between devices  44.1 us (43%)
  waiting for transfers between devices  26.5 us (26%)
  blocking collectives  18.7 us (18%)
  Pallas kernels  12.3 us (12%)
    ppermute x27, starting transfers between devices, shifted(): return lax.ppermute(value, axis, [(i, (i + step) % n) for i in range(n)])  35.5 us
    ppermute x27, waiting for transfers between devices, shifted(): return lax.ppermute(value, axis, [(i, (i + step) % n) for i in range(n)])  23.8 us
    all_to_all x1, blocking collectives, layer(): back = lax.all_to_all(partial.reshape(32, 8, 512), EP, 0, 0, tiled=True)  18.7 us
    all_to_all x1, starting transfers between devices, layer(): block = lax.all_to_all(sent, 'z', 0, 0, tiled=True).reshape(64, 2176)  8.16 us
    pallas_call x1, Pallas kernels, layer(): pl.pallas_call(mixer_kernel, in_specs=[HB] * 17, out_specs=[VM] * 12, out...  3.43 us
    ppermute x1, waiting for transfers between devices, layer(): far_half = lax.ppermute(near_half, 'y', [(0, 1), (1, 0), (2, 3), (3, 2)])  2.69 us
    pallas_call x1, Pallas kernels, layer(): pl.pallas_call(state_kernel, in_specs=[VM, VM, HB], out_specs=HB, out_sha...  2.57 us
  transfers between devices with their start and end apart: 29, of which 13 were waited for; matrix products, arithmetic and copies ran while one was open for 0% of the time, Pallas kernels for 6%

profile of v1, /device:TPU:1, one launch (start us, length us, event | category | flops | bytes accessed | tf_op | source)
XLA Modules:
  0.0 102.4 jit_solution(10085481671973526432)
XLA Ops:
  0.7 3.4 %mixer.1 = (bf16[8,2048]{1,0:T(8,128)(2,1)S(1)}, bf16[8,2048]{1,0:T(8,128)(2,1)S(1)}, f32[16,128]{1,0:T(8,128)S(1)}, f32[16,128]{1,0:T(8,128)S(1)}, bf16[224,512...) custom-call(s32[16]{0:T(128)} %lengths.1, ...), custom_call_target="tpu_custom_call" | custom-call | tf_op jit(solution)/shard_map/mixer/pallas_call | solution.py:353
  4.1 3.3 %collective-permute-start = (bf16[8,2048]{1,0:T(8,128)(2,1)S(1)}, bf16[8,2048]{1,0:T(8,128)(2,1)S(1)}, u32[]{:S(2)}, u32[]{:S(2)}) collective-permute-start(bf16[8,2048]{1,0:T(8,128)(2,1)S(1)} %get-tuple-element.39), channel_id=1, source_target_pairs={{0,1},{1,0},{2,3},{3,2},{4,5},{5,4},{6,7},{7,6},{8,9},{9,8},{10,11... | collective-permute-start | bytes 98312 | tf_op jit(solution)/shard_map/ppermute | solution.py:26
  7.4 0.9 collective-permute-done
  8.3 0.1 collective-permute-start.1
  8.4 2.2 %collective-permute-start.2 = (bf16[8,2048]{1,0:T(8,128)(2,1)S(1)}, bf16[8,2048]{1,0:T(8,128)(2,1)S(1)}, u32[]{:S(2)}, u32[]{:S(2)}) collective-permute-start(bf16[8,2048]{1,0:T(8,128)(2,1)S(1)} %add_convert_fusion.pair), channel_id=1, source_target_pairs={{0,4},{2,6},{4,0},{6,2},{1,5},{3,7},{5,1},{7,3},{8,12},{10,14},{12... | collective-permute-start | bytes 98312 | tf_op jit(solution)/shard_map/ppermute | solution.py:26
  10.6 1.1 %collective-permute-start.3 = (bf16[8,2048]{1,0:T(8,128)(2,1)S(1)}, bf16[8,2048]{1,0:T(8,128)(2,1)S(1)}, u32[]{:S(2)}, u32[]{:S(2)}) collective-permute-start(bf16[8,2048]{1,0:T(8,128)(2,1)S(1)} %add_convert_fusion.pair), channel_id=1, source_target_pairs={{0,6},{2,0},{4,2},{6,4},{1,7},{3,1},{5,3},{7,5},{8,14},{10,8},{12,... | collective-permute-start | bytes 98312 | tf_op jit(solution)/shard_map/ppermute | solution.py:26
  11.6 0.7 collective-permute-done.1.r1
  12.3 0.8 collective-permute-done.2.r2
  13.1 0.5 collective-permute-done.3.r3
  13.6 0.9 after.1
  14.6 8.2 %all-to-all-start = ((bf16[8,8,2176]{2,1,0:T(8,128)(2,1)}), bf16[8,8,2176]{2,1,0:T(8,128)(2,1)S(1)}, u32[]{:S(2)}, u32[]{:S(2)}) async-start(bf16[8,8,2176]{2,1,0:T(8,128)(2,1)} %get-tuple-element.46), calls=%async_computation | async-start | bytes 557056 | tf_op jit(solution)/shard_map/all_to_all | solution.py:415
  22.7 2.2 %collective-permute-start.10 = (bf16[32,2048]{1,0:T(8,128)(2,1)S(1)}, bf16[32,2048]{1,0:T(8,128)(2,1)S(1)}, u32[]{:S(2)}, u32[]{:S(2)}) collective-permute-start(bf16[32,2048]{1,0:T(8,128)(2,1)S(1)} %bitcast.32), channel_id=1, source_target_pairs={{0,1},{1,0},{2,3},{3,2},{4,5},{5,4},{6,7},{7,6},{8,9},{9,8},{10,11... | collective-permute-start | bytes 393224 | tf_op jit(solution)/shard_map/ppermute | solution.py:26
  24.9 0.3 collective-permute-start.12
  25.2 0.2 collective-permute-start.11
  25.4 3.5 %collective-permute-start.18 = (bf16[224,512]{1,0:T(8,128)(2,1)S(1)}, bf16[224,512]{1,0:T(8,128)(2,1)S(1)}, u32[]{:S(2)}, u32[]{:S(2)}) collective-permute-start(bf16[224,512]{1,0:T(8,128)(2,1)S(1)} %get-tuple-element.58), channel_id=1, source_target_pairs={{0,4},{2,6},{4,0},{6,2},{1,5},{3,7},{5,1},{7,3},{8,12},{10,14},{12... | collective-permute-start | bytes 688136 | tf_op jit(solution)/shard_map/ppermute | solution.py:26
  28.9 0.8 collective-permute-start.8
  29.7 3.5 %collective-permute-done.17.y1 = bf16[224,512]{1,0:T(8,128)(2,1)S(1)} collective-permute-done((bf16[224,512]{1,0:T(8,128)(2,1)S(1)}, bf16[224,512]{1,0:T(8,128)(2,1)S(1)}, u32[]{:S(2)}, u32[]{:S(2)}) %collective-permute-start.17) | collective-permute-done | bytes 229408 | tf_op jit(solution)/shard_map/ppermute | solution.py:26
  33.2 0.9 collective-permute-start.9
  34.1 4.8 %collective-permute-done.18.y2 = bf16[224,512]{1,0:T(8,128)(2,1)S(1)} collective-permute-done((bf16[224,512]{1,0:T(8,128)(2,1)S(1)}, bf16[224,512]{1,0:T(8,128)(2,1)S(1)}, u32[]{:S(2)}, u32[]{:S(2)}) %collective-permute-start.18) | collective-permute-done | bytes 229408 | tf_op jit(solution)/shard_map/ppermute | solution.py:26
  38.9 0.9 collective-permute-start.13
  39.8 1.2 %collective-permute-start.4 = (bf16[64,2176]{1,0:T(8,128)(2,1)S(1)}, bf16[64,2176]{1,0:T(8,128)(2,1)S(1)}, u32[]{:S(2)}, u32[]{:S(2)}) collective-permute-start(bf16[64,2176]{1,0:T(8,128)(2,1)S(1)} %bitcast.17), channel_id=1, source_target_pairs={{0,8},{8,16},{16,24},{24,0},{1,9},{9,17},{17,25},{25,1},{2,10},{10... | collective-permute-start | bytes 835592 | tf_op jit(solution)/shard_map/ppermute | solution.py:26
  41.1 1.5 %collective-permute-start.5 = (bf16[64,2176]{1,0:T(8,128)(2,1)S(1)}, bf16[64,2176]{1,0:T(8,128)(2,1)S(1)}, u32[]{:S(2)}, u32[]{:S(2)}) collective-permute-start(bf16[64,2176]{1,0:T(8,128)(2,1)S(1)} %bitcast.18), channel_id=1, source_target_pairs={{0,24},{8,0},{16,8},{24,16},{1,25},{9,1},{17,9},{25,17},{2,26},{10... | collective-permute-start | bytes 835592 | tf_op jit(solution)/shard_map/ppermute | solution.py:26
  42.5 1.6 %collective-permute-start.6 = (bf16[32,2176]{1,0:T(8,128)(2,1)S(1)}, bf16[32,2176]{1,0:T(8,128)(2,1)S(1)}, u32[]{:S(2)}, u32[]{:S(2)}) collective-permute-start(bf16[32,2176]{1,0:T(8,128)(2,1)S(1)} %constant_dynamic-slice_fusion), channel_id=1, source_target_pairs={{0,16},{8,24},{16,0},{24,8},{1,17},{9,25},{17,1},{25,9},{2,18},{10... | collective-permute-start | bytes 417800 | tf_op jit(solution)/shard_map/ppermute | solution.py:26
  44.2 1.2 %collective-permute-start.20 = (bf16[224,512]{1,0:T(8,128)(2,1)S(1)}, bf16[224,512]{1,0:T(8,128)(2,1)S(1)}, u32[]{:S(2)}, u32[]{:S(2)}) collective-permute-start(bf16[224,512]{1,0:T(8,128)(2,1)S(1)} %get-tuple-element.56.y0), channel_id=1, source_target_pairs={{0,1},{1,0},{2,3},{3,2},{4,5},{5,4},{6,7},{7,6},{8,9},{9,8},{10,11... | collective-permute-start | bytes 688136 | tf_op jit(solution)/shard_map/ppermute | solution.py:26
  45.4 0.3 collective-permute-start.21
  45.6 7.3 %collective-permute-done.6.near_half = bf16[32,2176]{1,0:T(8,128)(2,1)S(1)} collective-permute-done((bf16[32,2176]{1,0:T(8,128)(2,1)S(1)}, bf16[32,2176]{1,0:T(8,128)(2,1)S(1)}, u32[]{:S(2)}, u32[]{:S(2)}) %collective-permute-start.6) | collective-permute-done | bytes 139296 | tf_op jit(solution)/shard_map/ppermute | solution.py:26
  52.9 1.2 %collective-permute-start.22 = (bf16[224,512]{1,0:T(8,128)(2,1)S(1)}, bf16[224,512]{1,0:T(8,128)(2,1)S(1)}, u32[]{:S(2)}, u32[]{:S(2)}) collective-permute-start(bf16[224,512]{1,0:T(8,128)(2,1)S(1)} %collective-permute-done.18.y2), channel_id=1, source_target_pairs={{0,1},{1,0},{2,3},{3,2},{4,5},{5,4},{6,7},{7,6},{8,9},{9,8},{10,11... | collective-permute-start | bytes 688136 | tf_op jit(solution)/shard_map/ppermute | solution.py:26
  54.1 0.5 collective-permute-start.7
  54.6 1.7 %pack.1.w_all = bf16[1024,2048]{1,0:T(8,128)(2,1)S(1)} custom-call(bf16[2,64,2048]{2,1,0:T(8,128)(2,1)} %bitcast.26, bf16[2,64,2048]{2,1,0:T(8,128)(2,1)} %bitcast.28, bf16[32,2048]{1,0:T(8,128)(2,1)} %bitcast.31, bf16[32,2048]{1,0:T(8,128)(2,1)} %bitcast.33, bf16[64,2048]{1,0:T(8,128)(2,1)} %bitcast.4.refs_4_, bf16[64,2048]{1,0:T(8,128)(2,1)} %bitcast.30, ...), custom_call_target="tpu_custom_call" | custom-call | tf_op jit(solution)/shard_map/pack/pallas_call | solution.py:421
  56.3 2.7 %collective-permute-done.7.far_half = bf16[32,2176]{1,0:T(8,128)(2,1)S(1)} collective-permute-done((bf16[32,2176]{1,0:T(8,128)(2,1)S(1)}, bf16[32,2176]{1,0:T(8,128)(2,1)S(1)}, u32[]{:S(2)}, u32[]{:S(2)}) %collective-permute-start.7) | collective-permute-done | bytes 139296 | tf_op jit(solution)/shard_map/ppermute | solution.py:418
  59.0 1.9 %hidden.1 = (bf16[272,128]{1,0:T(8,128)(2,1)S(1)}, bf16[256,128]{1,0:T(8,128)(2,1)S(1)}) custom-call(bf16[64,2176]{1,0:T(8,128)(2,1)S(1)} %bitcast.20, bf16[64,2176]{1,0:T(8,128)(2,1)S(1)} %collective-permute-done.4.b1, bf16[64,2176]{1,0:T(8,128)(2,1)S(1)} %collective-permute-done.5.b3, bf16[32,2176]{1,0:T(8,128)(2,1)S(1)} %collective-permute-done.6.near_half, ...), custom_call_target="tpu_custom_call" | custom-call | tf_op jit(solution)/shard_map/hidden/pallas_call | solution.py:444
  60.9 0.5 collective-permute-start.14
  61.4 3.0 %collective-permute-start.15 = (bf16[272,128]{1,0:T(8,128)(2,1)S(1)}, bf16[272,128]{1,0:T(8,128)(2,1)S(1)}, u32[]{:S(2)}, u32[]{:S(2)}) collective-permute-start(bf16[272,128]{1,0:T(8,128)(2,1)S(1)} %get-tuple-element.54.h0), channel_id=1, source_target_pairs={{0,4},{2,6},{4,0},{6,2},{1,5},{3,7},{5,1},{7,3},{8,12},{10,14},{12... | collective-permute-start | bytes 208904 | tf_op jit(solution)/shard_map/ppermute | solution.py:26
  64.4 0.9 collective-permute-start.16
  65.3 0.1 arrange.1.d_all
  65.4 1.4 %collective-permute-done.15.h2 = bf16[272,128]{1,0:T(8,128)(2,1)S(1)} collective-permute-done((bf16[272,128]{1,0:T(8,128)(2,1)S(1)}, bf16[272,128]{1,0:T(8,128)(2,1)S(1)}, u32[]{:S(2)}, u32[]{:S(2)}) %collective-permute-start.15) | collective-permute-done | bytes 69664 | tf_op jit(solution)/shard_map/ppermute | solution.py:26
  66.9 1.3 %collective-permute-done.16.h3 = bf16[272,128]{1,0:T(8,128)(2,1)S(1)} collective-permute-done((bf16[272,128]{1,0:T(8,128)(2,1)S(1)}, bf16[272,128]{1,0:T(8,128)(2,1)S(1)}, u32[]{:S(2)}, u32[]{:S(2)}) %collective-permute-start.16) | collective-permute-done | bytes 69664 | tf_op jit(solution)/shard_map/ppermute | solution.py:26
  68.2 0.7 down.1
  68.9 18.7 %all_to_all.10.back = bf16[32,8,512]{2,1,0:T(8,128)(2,1)S(1)} all-to-all(bf16[32,8,512]{2,1,0:T(8,128)(2,1)S(1)} %bitcast.21), channel_id=1, replica_groups=mesh['z'=8,'x'=4,'y'=4,'c'=2] {'z','x'}, dimensions={0} | all-to-all | bytes 524288 | tf_op jit(solution)/shard_map/all_to_all | solution.py:476
  87.7 0.1 collective-permute-start.24
  87.8 3.0 %collective-permute-start.25 = (f32[8,512]{1,0:T(8,128)S(1)}, f32[8,512]{1,0:T(8,128)S(1)}, u32[]{:S(2)}, u32[]{:S(2)}) collective-permute-start(f32[8,512]{1,0:T(8,128)S(1)} %sum.1.s0), channel_id=1, source_target_pairs={{0,4},{2,6},{4,0},{6,2},{1,5},{3,7},{5,1},{7,3},{8,12},{10,14},{12... | collective-permute-start | bytes 49160 | tf_op jit(solution)/shard_map/ppermute | solution.py:26
  90.8 0.8 collective-permute-done.24.s1
  91.6 0.5 collective-permute-done.25.s2
  92.1 1.3 %collective-permute-done.26.s3 = f32[8,512]{1,0:T(8,128)S(1)} collective-permute-done((f32[8,512]{1,0:T(8,128)S(1)}, f32[8,512]{1,0:T(8,128)S(1)}, u32[]{:S(2)}, u32[]{:S(2)}) %collective-permute-start.26) | collective-permute-done | bytes 16416 | tf_op jit(solution)/shard_map/ppermute | solution.py:26
  93.4 0.2 last.1.own
  93.6 5.6 %collective-permute-start.27 = (bf16[8,2048]{1,0:T(8,128)(2,1)S(1)}, bf16[8,2048]{1,0:T(8,128)(2,1)S(1)}, u32[]{:S(2)}, u32[]{:S(2)}) collective-permute-start(bf16[8,2048]{1,0:T(8,128)(2,1)S(1)} %last.1.own), channel_id=1, source_target_pairs={{0,1},{1,0},{2,3},{3,2},{4,5},{5,4},{6,7},{7,6},{8,9},{9,8},{10,11... | collective-permute-start | bytes 98312 | tf_op jit(solution)/shard_map/ppermute | solution.py:26
  99.2 2.6 %state.1 = f32[16,128,128]{2,1,0:T(8,128)} custom-call(f32[16,128]{1,0:T(8,128)S(1)} %get-tuple-element.64.keys, f32[16,128]{1,0:T(8,128)S(1)} %get-tuple-element.65.values, f32[16,128,128]{2,1,0:T(8,128)} %bitcast.23), custom_call_target="tpu_custom_call" | custom-call | tf_op jit(solution)/shard_map/state/pallas_call | solution.py:430
  101.8 0.6 join.1
  (30 shorter events, 0.1 us)
Async XLA Ops:
  0.6 7.6 %copy-start.2 = (bf16[2048]{0:T(1024)(128)(2,1)S(1)}, bf16[2048]{0:T(1024)(128)(2,1)}, u32[]{:S(2)}) copy-start(bf16[2048]{0:T(1024)(128)(2,1)} %param.42) | copy-start | bytes 12292
  0.6 22.1 %copy-start = (bf16[2048,32]{0,1:T(8,128)(2,1)S(1)}, bf16[2048,32]{0,1:T(8,128)(2,1)}, u32[]{:S(2)}) copy-start(bf16[2048,32]{0,1:T(8,128)(2,1)} %param.43) | copy-start | bytes 393220
  0.7 24.5 %copy-start.1 = (bf16[2048,32]{0,1:T(8,128)(2,1)S(1)}, bf16[2048,32]{0,1:T(8,128)(2,1)}, u32[]{:S(2)}) copy-start(bf16[2048,32]{0,1:T(8,128)(2,1)} %param.44) | copy-start | bytes 393220
  4.1 4.1 %collective-permute-start = (bf16[8,2048]{1,0:T(8,128)(2,1)S(1)}, bf16[8,2048]{1,0:T(8,128)(2,1)S(1)}, u32[]{:S(2)}, u32[]{:S(2)}) collective-permute-start(bf16[8,2048]{1,0:T(8,128)(2,1)S(1)} %get-tuple-element.39), channel_id=1, source_target_pairs={{0,1},{1,0},{2,3},{3,2},{4,5},{5,4},{6,7},{7,6},{8,9},{9,8},{10,11... | collective-permute-start | bytes 98312 | tf_op jit(solution)/shard_map/ppermute | solution.py:26
  8.3 4.1 %collective-permute-start.1 = (bf16[8,2048]{1,0:T(8,128)(2,1)S(1)}, bf16[8,2048]{1,0:T(8,128)(2,1)S(1)}, u32[]{:S(2)}, u32[]{:S(2)}) collective-permute-start(bf16[8,2048]{1,0:T(8,128)(2,1)S(1)} %add_convert_fusion.pair), channel_id=1, source_target_pairs={{0,2},{2,4},{4,6},{6,0},{1,3},{3,5},{5,7},{7,1},{8,10},{10,12},{12... | collective-permute-start | bytes 98312 | tf_op jit(solution)/shard_map/ppermute | solution.py:26
  8.4 4.8 %collective-permute-start.2 = (bf16[8,2048]{1,0:T(8,128)(2,1)S(1)}, bf16[8,2048]{1,0:T(8,128)(2,1)S(1)}, u32[]{:S(2)}, u32[]{:S(2)}) collective-permute-start(bf16[8,2048]{1,0:T(8,128)(2,1)S(1)} %add_convert_fusion.pair), channel_id=1, source_target_pairs={{0,4},{2,6},{4,0},{6,2},{1,5},{3,7},{5,1},{7,3},{8,12},{10,14},{12... | collective-permute-start | bytes 98312 | tf_op jit(solution)/shard_map/ppermute | solution.py:26
  10.6 3.1 %collective-permute-start.3 = (bf16[8,2048]{1,0:T(8,128)(2,1)S(1)}, bf16[8,2048]{1,0:T(8,128)(2,1)S(1)}, u32[]{:S(2)}, u32[]{:S(2)}) collective-permute-start(bf16[8,2048]{1,0:T(8,128)(2,1)S(1)} %add_convert_fusion.pair), channel_id=1, source_target_pairs={{0,6},{2,0},{4,2},{6,4},{1,7},{3,1},{5,3},{7,5},{8,14},{10,8},{12,... | collective-permute-start | bytes 98312 | tf_op jit(solution)/shard_map/ppermute | solution.py:26
  14.6 25.3 %all-to-all-start = ((bf16[8,8,2176]{2,1,0:T(8,128)(2,1)}), bf16[8,8,2176]{2,1,0:T(8,128)(2,1)S(1)}, u32[]{:S(2)}, u32[]{:S(2)}) async-start(bf16[8,8,2176]{2,1,0:T(8,128)(2,1)} %get-tuple-element.46), calls=%async_computation | async-start | bytes 557056 | tf_op jit(solution)/shard_map/all_to_all | solution.py:415
  22.7 6.1 %collective-permute-start.10 = (bf16[32,2048]{1,0:T(8,128)(2,1)S(1)}, bf16[32,2048]{1,0:T(8,128)(2,1)S(1)}, u32[]{:S(2)}, u32[]{:S(2)}) collective-permute-start(bf16[32,2048]{1,0:T(8,128)(2,1)S(1)} %bitcast.32), channel_id=1, source_target_pairs={{0,1},{1,0},{2,3},{3,2},{4,5},{5,4},{6,7},{7,6},{8,9},{9,8},{10,11... | collective-permute-start | bytes 393224 | tf_op jit(solution)/shard_map/ppermute | solution.py:26
  24.9 8.3 %collective-permute-start.17 = (bf16[224,512]{1,0:T(8,128)(2,1)S(1)}, bf16[224,512]{1,0:T(8,128)(2,1)S(1)}, u32[]{:S(2)}, u32[]{:S(2)}) collective-permute-start(bf16[224,512]{1,0:T(8,128)(2,1)S(1)} %get-tuple-element.57), channel_id=1, source_target_pairs={{0,2},{2,4},{4,6},{6,0},{1,3},{3,5},{5,7},{7,1},{8,10},{10,12},{12... | collective-permute-start | bytes 688136 | tf_op jit(solution)/shard_map/ppermute | solution.py:26
  24.9 16.1 %collective-permute-start.12 = (bf16[64,2048]{1,0:T(8,128)(2,1)}, bf16[64,2048]{1,0:T(8,128)(2,1)S(1)}, u32[]{:S(2)}, u32[]{:S(2)}) collective-permute-start(bf16[64,2048]{1,0:T(8,128)(2,1)} %bitcast.4.refs_4_), channel_id=1, source_target_pairs={{0,1},{1,0},{2,3},{3,2},{4,5},{5,4},{6,7},{7,6},{8,9},{9,8},{10,11... | collective-permute-start | bytes 786440 | tf_op jit(solution)/shard_map/ppermute | solution.py:26
  25.2 3.7 %collective-permute-start.11 = (bf16[32,2048]{1,0:T(8,128)(2,1)S(1)}, bf16[32,2048]{1,0:T(8,128)(2,1)S(1)}, u32[]{:S(2)}, u32[]{:S(2)}) collective-permute-start(bf16[32,2048]{1,0:T(8,128)(2,1)S(1)} %bitcast.34), channel_id=1, source_target_pairs={{0,1},{1,0},{2,3},{3,2},{4,5},{5,4},{6,7},{7,6},{8,9},{9,8},{10,11... | collective-permute-start | bytes 393224 | tf_op jit(solution)/shard_map/ppermute | solution.py:26
  25.4 13.5 %collective-permute-start.18 = (bf16[224,512]{1,0:T(8,128)(2,1)S(1)}, bf16[224,512]{1,0:T(8,128)(2,1)S(1)}, u32[]{:S(2)}, u32[]{:S(2)}) collective-permute-start(bf16[224,512]{1,0:T(8,128)(2,1)S(1)} %get-tuple-element.58), channel_id=1, source_target_pairs={{0,4},{2,6},{4,0},{6,2},{1,5},{3,7},{5,1},{7,3},{8,12},{10,14},{12... | collective-permute-start | bytes 688136 | tf_op jit(solution)/shard_map/ppermute | solution.py:26
  28.9 11.0 %collective-permute-start.19 = (bf16[224,512]{1,0:T(8,128)(2,1)S(1)}, bf16[224,512]{1,0:T(8,128)(2,1)S(1)}, u32[]{:S(2)}, u32[]{:S(2)}) collective-permute-start(bf16[224,512]{1,0:T(8,128)(2,1)S(1)} %get-tuple-element.59), channel_id=1, source_target_pairs={{0,6},{2,0},{4,2},{6,4},{1,7},{3,1},{5,3},{7,5},{8,14},{10,8},{12,... | collective-permute-start | bytes 688136 | tf_op jit(solution)/shard_map/ppermute | solution.py:26
  28.9 15.3 %collective-permute-start.8 = (bf16[2,64,2048]{2,1,0:T(8,128)(2,1)}, bf16[2,64,2048]{2,1,0:T(8,128)(2,1)S(1)}, u32[]{:S(2)}, u32[]{:S(2)}) collective-permute-start(bf16[2,64,2048]{2,1,0:T(8,128)(2,1)} %bitcast.25), channel_id=1, source_target_pairs={{0,1},{1,0},{2,3},{3,2},{4,5},{5,4},{6,7},{7,6},{8,9},{9,8},{10,11... | collective-permute-start | bytes 1572872 | tf_op jit(solution)/shard_map/ppermute | solution.py:26
  33.2 12.2 %collective-permute-start.9 = (bf16[2,64,2048]{2,1,0:T(8,128)(2,1)}, bf16[2,64,2048]{2,1,0:T(8,128)(2,1)S(1)}, u32[]{:S(2)}, u32[]{:S(2)}) collective-permute-start(bf16[2,64,2048]{2,1,0:T(8,128)(2,1)} %bitcast.27), channel_id=1, source_target_pairs={{0,1},{1,0},{2,3},{3,2},{4,5},{5,4},{6,7},{7,6},{8,9},{9,8},{10,11... | collective-permute-start | bytes 1572872 | tf_op jit(solution)/shard_map/ppermute | solution.py:26
  38.9 3.7 %collective-permute-start.13 = (bf16[64,2048]{1,0:T(8,128)(2,1)}, bf16[64,2048]{1,0:T(8,128)(2,1)S(1)}, u32[]{:S(2)}, u32[]{:S(2)}) collective-permute-start(bf16[64,2048]{1,0:T(8,128)(2,1)} %bitcast.29), channel_id=1, source_target_pairs={{0,1},{1,0},{2,3},{3,2},{4,5},{5,4},{6,7},{7,6},{8,9},{9,8},{10,11... | collective-permute-start | bytes 786440 | tf_op jit(solution)/shard_map/ppermute | solution.py:26
  39.8 14.3 %collective-permute-start.4 = (bf16[64,2176]{1,0:T(8,128)(2,1)S(1)}, bf16[64,2176]{1,0:T(8,128)(2,1)S(1)}, u32[]{:S(2)}, u32[]{:S(2)}) collective-permute-start(bf16[64,2176]{1,0:T(8,128)(2,1)S(1)} %bitcast.17), channel_id=1, source_target_pairs={{0,8},{8,16},{16,24},{24,0},{1,9},{9,17},{17,25},{25,1},{2,10},{10... | collective-permute-start | bytes 835592 | tf_op jit(solution)/shard_map/ppermute | solution.py:26
  41.1 13.0 %collective-permute-start.5 = (bf16[64,2176]{1,0:T(8,128)(2,1)S(1)}, bf16[64,2176]{1,0:T(8,128)(2,1)S(1)}, u32[]{:S(2)}, u32[]{:S(2)}) collective-permute-start(bf16[64,2176]{1,0:T(8,128)(2,1)S(1)} %bitcast.18), channel_id=1, source_target_pairs={{0,24},{8,0},{16,8},{24,16},{1,25},{9,1},{17,9},{25,17},{2,26},{10... | collective-permute-start | bytes 835592 | tf_op jit(solution)/shard_map/ppermute | solution.py:26
  42.5 10.3 %collective-permute-start.6 = (bf16[32,2176]{1,0:T(8,128)(2,1)S(1)}, bf16[32,2176]{1,0:T(8,128)(2,1)S(1)}, u32[]{:S(2)}, u32[]{:S(2)}) collective-permute-start(bf16[32,2176]{1,0:T(8,128)(2,1)S(1)} %constant_dynamic-slice_fusion), channel_id=1, source_target_pairs={{0,16},{8,24},{16,0},{24,8},{1,17},{9,25},{17,1},{25,9},{2,18},{10... | collective-permute-start | bytes 417800 | tf_op jit(solution)/shard_map/ppermute | solution.py:26
  44.2 17.3 %collective-permute-start.20 = (bf16[224,512]{1,0:T(8,128)(2,1)S(1)}, bf16[224,512]{1,0:T(8,128)(2,1)S(1)}, u32[]{:S(2)}, u32[]{:S(2)}) collective-permute-start(bf16[224,512]{1,0:T(8,128)(2,1)S(1)} %get-tuple-element.56.y0), channel_id=1, source_target_pairs={{0,1},{1,0},{2,3},{3,2},{4,5},{5,4},{6,7},{7,6},{8,9},{9,8},{10,11... | collective-permute-start | bytes 688136 | tf_op jit(solution)/shard_map/ppermute | solution.py:26
  45.4 19.0 %collective-permute-start.21 = (bf16[224,512]{1,0:T(8,128)(2,1)S(1)}, bf16[224,512]{1,0:T(8,128)(2,1)S(1)}, u32[]{:S(2)}, u32[]{:S(2)}) collective-permute-start(bf16[224,512]{1,0:T(8,128)(2,1)S(1)} %collective-permute-done.17.y1), channel_id=1, source_target_pairs={{0,1},{1,0},{2,3},{3,2},{4,5},{5,4},{6,7},{7,6},{8,9},{9,8},{10,11... | collective-permute-start | bytes 688136 | tf_op jit(solution)/shard_map/ppermute | solution.py:26
  52.9 12.4 %collective-permute-start.22 = (bf16[224,512]{1,0:T(8,128)(2,1)S(1)}, bf16[224,512]{1,0:T(8,128)(2,1)S(1)}, u32[]{:S(2)}, u32[]{:S(2)}) collective-permute-start(bf16[224,512]{1,0:T(8,128)(2,1)S(1)} %collective-permute-done.18.y2), channel_id=1, source_target_pairs={{0,1},{1,0},{2,3},{3,2},{4,5},{5,4},{6,7},{7,6},{8,9},{9,8},{10,11... | collective-permute-start | bytes 688136 | tf_op jit(solution)/shard_map/ppermute | solution.py:26
  54.1 11.2 %collective-permute-start.23 = (bf16[224,512]{1,0:T(8,128)(2,1)S(1)}, bf16[224,512]{1,0:T(8,128)(2,1)S(1)}, u32[]{:S(2)}, u32[]{:S(2)}) collective-permute-start(bf16[224,512]{1,0:T(8,128)(2,1)S(1)} %collective-permute-done.19.y3), channel_id=1, source_target_pairs={{0,1},{1,0},{2,3},{3,2},{4,5},{5,4},{6,7},{7,6},{8,9},{9,8},{10,11... | collective-permute-start | bytes 688136 | tf_op jit(solution)/shard_map/ppermute | solution.py:26
  54.1 4.9 %collective-permute-start.7 = (bf16[32,2176]{1,0:T(8,128)(2,1)S(1)}, bf16[32,2176]{1,0:T(8,128)(2,1)S(1)}, u32[]{:S(2)}, u32[]{:S(2)}) collective-permute-start(bf16[32,2176]{1,0:T(8,128)(2,1)S(1)} %collective-permute-done.6.near_half), channel_id=1, source_target_pairs={{0,2},{2,0},{4,6},{6,4},{1,3},{3,1},{5,7},{7,5},{8,10},{10,8},{12,... | collective-permute-start | bytes 417800 | tf_op jit(solution)/shard_map/ppermute | solution.py:418
  60.9 4.5 %collective-permute-start.14 = (bf16[272,128]{1,0:T(8,128)(2,1)S(1)}, bf16[272,128]{1,0:T(8,128)(2,1)S(1)}, u32[]{:S(2)}, u32[]{:S(2)}) collective-permute-start(bf16[272,128]{1,0:T(8,128)(2,1)S(1)} %get-tuple-element.54.h0), channel_id=1, source_target_pairs={{0,2},{2,4},{4,6},{6,0},{1,3},{3,5},{5,7},{7,1},{8,10},{10,12},{12... | collective-permute-start | bytes 208904 | tf_op jit(solution)/shard_map/ppermute | solution.py:26
  61.4 5.4 %collective-permute-start.15 = (bf16[272,128]{1,0:T(8,128)(2,1)S(1)}, bf16[272,128]{1,0:T(8,128)(2,1)S(1)}, u32[]{:S(2)}, u32[]{:S(2)}) collective-permute-start(bf16[272,128]{1,0:T(8,128)(2,1)S(1)} %get-tuple-element.54.h0), channel_id=1, source_target_pairs={{0,4},{2,6},{4,0},{6,2},{1,5},{3,7},{5,1},{7,3},{8,12},{10,14},{12... | collective-permute-start | bytes 208904 | tf_op jit(solution)/shard_map/ppermute | solution.py:26
  64.4 3.8 %collective-permute-start.16 = (bf16[272,128]{1,0:T(8,128)(2,1)S(1)}, bf16[272,128]{1,0:T(8,128)(2,1)S(1)}, u32[]{:S(2)}, u32[]{:S(2)}) collective-permute-start(bf16[272,128]{1,0:T(8,128)(2,1)S(1)} %get-tuple-element.54.h0), channel_id=1, source_target_pairs={{0,6},{2,0},{4,2},{6,4},{1,7},{3,1},{5,3},{7,5},{8,14},{10,8},{12,... | collective-permute-start | bytes 208904 | tf_op jit(solution)/shard_map/ppermute | solution.py:26
  87.7 3.9 %collective-permute-start.24 = (f32[8,512]{1,0:T(8,128)S(1)}, f32[8,512]{1,0:T(8,128)S(1)}, u32[]{:S(2)}, u32[]{:S(2)}) collective-permute-start(f32[8,512]{1,0:T(8,128)S(1)} %sum.1.s0), channel_id=1, source_target_pairs={{0,2},{2,4},{4,6},{6,0},{1,3},{3,5},{5,7},{7,1},{8,10},{10,12},{12... | collective-permute-start | bytes 49160 | tf_op jit(solution)/shard_map/ppermute | solution.py:26
  87.8 4.3 %collective-permute-start.25 = (f32[8,512]{1,0:T(8,128)S(1)}, f32[8,512]{1,0:T(8,128)S(1)}, u32[]{:S(2)}, u32[]{:S(2)}) collective-permute-start(f32[8,512]{1,0:T(8,128)S(1)} %sum.1.s0), channel_id=1, source_target_pairs={{0,4},{2,6},{4,0},{6,2},{1,5},{3,7},{5,1},{7,3},{8,12},{10,14},{12... | collective-permute-start | bytes 49160 | tf_op jit(solution)/shard_map/ppermute | solution.py:26
  90.8 2.6 %collective-permute-start.26 = (f32[8,512]{1,0:T(8,128)S(1)}, f32[8,512]{1,0:T(8,128)S(1)}, u32[]{:S(2)}, u32[]{:S(2)}) collective-permute-start(f32[8,512]{1,0:T(8,128)S(1)} %sum.1.s0), channel_id=1, source_target_pairs={{0,6},{2,0},{4,2},{6,4},{1,7},{3,1},{5,3},{7,5},{8,14},{10,8},{12,... | collective-permute-start | bytes 49160 | tf_op jit(solution)/shard_map/ppermute | solution.py:26
  93.6 8.2 %collective-permute-start.27 = (bf16[8,2048]{1,0:T(8,128)(2,1)S(1)}, bf16[8,2048]{1,0:T(8,128)(2,1)S(1)}, u32[]{:S(2)}, u32[]{:S(2)}) collective-permute-start(bf16[8,2048]{1,0:T(8,128)(2,1)S(1)} %last.1.own), channel_id=1, source_target_pairs={{0,1},{1,0},{2,3},{3,2},{4,5},{5,4},{6,7},{7,6},{8,9},{9,8},{10,11... | collective-permute-start | bytes 98312 | tf_op jit(solution)/shard_map/ppermute | solution.py:26

commit v2 on v1

--- a/solution.py
+++ b/solution.py
@@ -56,8 +56,8 @@
 
 
 def mixer_kernel(
-    lengths, frequency, tokens, gain, wq, wk, wv, wg, state, ow, ed, dd, sd, ids, ews, gain1, gain2,
-    kept, given, key_out, value_out, d0, d1, d2, d3, mine, info, g1, g2,
+    lengths, frequency, tokens, gain, wq, wk, wv, wg, state, ow, ed, dd, sd, ids, ews, gain1,
+    kept, given, key_out, value_out, d0, d1, d2, d3, mine, info, g1,
     bl, bf, bt, bn, bq, bk, bv, bg, bs, bo, bi, bw, rows, table, sems, dsems,
 ):
     moves = [
@@ -66,11 +66,11 @@
             (
                 (wq, bq), (wk, bk), (state, bs), (wv, bv), (wg, bg), (ow, bo),
                 (lengths, bl), (frequency, bf), (tokens, bt), (gain, bn),
-                (ids, bi), (ews, bw), (gain1, g1), (gain2, g2),
+                (ids, bi), (ews, bw), (gain1, g1),
             )
         )
     ]
-    for i in (6, 7, 8, 0, 1, 2, 3, 4, 5, 9, 10, 11, 12, 13):
+    for i in (6, 7, 8, 0, 1, 2, 3, 4, 5, 9, 10, 11, 12):
         moves[i].start()
     slices = []
     for k, out in enumerate((d0, d1, d2, d3)):
@@ -136,7 +136,7 @@
     table[16:22, 0:16] = w - top
     f = table[...].T
     info[...] = jnp.where(first, f[0:8], f[8:16]).astype(BF)
-    for c in (moves[12], moves[13], *slices):
+    for c in (moves[12], *slices):
         c.wait()
 
 
@@ -161,7 +161,9 @@
         c.wait()
 
 
-def arrange_kernel(y0, y1, y2, y3, p0, p1, p2, p3, out):
+def arrange_kernel(y0, y1, y2, y3, p0, p1, p2, p3, gain, out, gain_out, sem):
+    move = pltpu.make_async_copy(gain, gain_out, sem.at[0])
+    move.start()
     for k, pair in enumerate(((y0, p0), (y1, p1), (y2, p2), (y3, p3))):
         for s, src in enumerate(pair):
             for j in range(3):
@@ -169,6 +171,7 @@
                 out[o : o + 64, :] = src[64 * j : 64 * j + 64, :]
             o = 1536 + 64 * k + 32 * s
             out[o : o + 32, :] = src[192:224, :]
+    move.wait()
 
 
 def state_kernel(keys, values, state, new_state, bs, bn, sems):
@@ -292,19 +295,20 @@
     out[...] = total
 
 
-def last_kernel(s0, s1, s2, s3, after, gain, out, whole):
+def both_kernel(own, other, out):
+    first = lax.axis_index("c") == 0
+    out[0:8] = jnp.where(first, own[...], other[...])
+    out[8:16] = jnp.where(first, other[...], own[...])
+
+
+def last_kernel(s0, s1, s2, s3, own, other, gain, out, whole):
     for k, s in enumerate((s0, s1, s2, s3)):
         start = lax.rem(lax.axis_index("y") + 4 - k, 4) * 512
         whole[:, pl.ds(pl.multiple_of(start, 512), 512)] = s[...]
-    out[...] = norm(RESIDUAL_SCALE * after[...].astype(F32) + whole[...], gain[...]).astype(BF)
-
-
-def join_kernel(own, other, out):
     first = lax.axis_index("c") == 0
     a, b = own[...].astype(F32), other[...].astype(F32)
-    low = jnp.where(first, a, b)
-    high = jnp.where(first, b, a)
-    out[...] = jnp.concatenate([low, high], axis=0).astype(BF)
+    rows = jnp.concatenate([jnp.where(first, a, b), jnp.where(first, b, a)], axis=0)
+    out[...] = norm(RESIDUAL_SCALE * rows + whole[...], gain[...]).astype(BF)
 
 
 def limit(mib):
@@ -352,13 +356,12 @@
     state = old_state.reshape(16, 128, 128)
     outs = pl.pallas_call(
         mixer_kernel,
-        in_specs=[HB] * 17,
-        out_specs=[VM] * 12,
+        in_specs=[HB] * 16,
+        out_specs=[VM] * 11,
         out_shape=[shape(8, 2048)] * 2
         + [shape(16, 128, dtype=F32)] * 2
         + [shape(224, 512)] * 4
-        + [shape(8, 2048), shape(8, 128)]
-        + [shape(1, 2048, dtype=F32)] * 2,
+        + [shape(8, 2048), shape(8, 128), shape(1, 2048, dtype=F32)],
         scratch_shapes=[
             pltpu.SMEM((16,), jnp.int32),
             pltpu.VMEM((1, 128), F32),
@@ -373,7 +376,7 @@
             pltpu.VMEM((6, 16), F32),
             pltpu.VMEM((16, 128), F32),
             pltpu.VMEM((128, 128), F32),
-            pltpu.SemaphoreType.DMA((14,)),
+            pltpu.SemaphoreType.DMA((13,)),
             pltpu.SemaphoreType.DMA((16,)),
         ],
         compiler_params=limit(8),
@@ -385,12 +388,12 @@
                 lengths, jnp.asarray(frequency)[None], tokens, head_gain.reshape(1, 128),
                 query_weight, key_weight, value_weight, gate_weight, state, output_weight,
                 expert_down, dense_down, shared_down, expert_ids.T, expert_weights.T,
-                first_gain.reshape(1, 2048), second_gain.reshape(1, 2048),
+                first_gain.reshape(1, 2048),
             )
         ]
     )
     kept, given, keys, values = outs[0:4]
-    downs, (mine, info, g1, g2) = outs[4:8], outs[8:12]
+    downs, (mine, info, g1) = outs[4:8], outs[8:11]
 
     pair = (kept.astype(F32) + shifted(given, "c", 1).astype(F32)).astype(BF)
     raw = (
@@ -398,21 +401,22 @@
         dense_gate.T, dense_up.T, shared_gate.T, shared_up.T,
     )
     side = jnp.broadcast_to(side_gate[None], (8, 2048))
-    side, downs, pair = lax.optimization_barrier((side, downs, pair))
+    side, downs, raw, pair = lax.optimization_barrier((side, downs, raw, pair))
     arrived = [shifted(pair, "y", k) for k in range(1, 4)]
+    peers = [shifted(r, "c", 1) for r in raw]
     from_y = [downs[0]] + [shifted(downs[k], "y", k) for k in range(1, 4)]
     after, sent = pl.pallas_call(
         after_kernel,
         in_specs=[VM] * 7,
         out_specs=[VM, VM],
-        out_shape=[shape(8, 2048), jax.ShapeDtypeStruct((8, 8, 2176), BF)],
+        out_shape=[shape(8, 2048), shape(8, 8, 2176)],
         compiler_params=limit(4),
         name="after",
     )(pair, *arrived, mine, g1, info)
 
-    raw, side, sent = lax.optimization_barrier((raw, side, sent))
-    peers = [shifted(r, "c", 1) for r in raw]
+    side, sent = lax.optimization_barrier((side, sent))
     block = lax.all_to_all(sent, "z", 0, 0, tiled=True).reshape(64, 2176)
+    other = shifted(after, "c", 1)
     part = lax.dynamic_slice_in_dim(block, (lax.axis_index("y") % 2) * 32, 32, 0)
     near_half = shifted(part, "x", 2)
     far_half = lax.ppermute(near_half, "y", [(0, 1), (1, 0), (2, 3), (3, 2)])
@@ -455,15 +459,17 @@
         compiler_params=limit(8),
         name="hidden",
     )(*blocks, near(w_all), side)
-    gathered = [hidden] + [shifted(hidden, "y", k) for k in range(1, 4)]
-    d_all = pl.pallas_call(
+    h2, h1, h3 = (shifted(hidden, "y", k) for k in (2, 1, 3))
+    gathered = [hidden, h1, h2, h3]
+    d_all, g2 = pl.pallas_call(
         arrange_kernel,
-        in_specs=[VM] * 8,
-        out_specs=VM,
-        out_shape=shape(1792, 512),
+        in_specs=[VM] * 8 + [HB],
+        out_specs=[VM, VM],
+        out_shape=[shape(1792, 512), shape(1, 2048, dtype=F32)],
+        scratch_shapes=[pltpu.SemaphoreType.DMA((1,))],
         compiler_params=limit(2),
         name="arrange",
-    )(*from_y, *from_c)
+    )(*from_y, *from_c, big(second_gain.reshape(1, 2048)))
     partial, shared = pl.pallas_call(
         down_kernel,
         in_specs=[VM] * 6,
@@ -482,24 +488,24 @@
         compiler_params=limit(3),
         name="sum",
     )(back, shared)
-    pieces = [total] + [shifted(total, "y", k) for k in range(1, 4)]
-    final = pl.pallas_call(
+    both = pl.pallas_call(
+        both_kernel,
+        in_specs=[VM] * 2,
+        out_specs=VM,
+        out_shape=shape(16, 512, dtype=F32),
+        compiler_params=limit(3),
+        name="both",
+    )(total, shifted(total, "c", 1))
+    s2, s1, s3 = (shifted(both, "y", k) for k in (2, 1, 3))
+    layer_out = pl.pallas_call(
         last_kernel,
-        in_specs=[VM] * 6,
+        in_specs=[VM] * 7,
         out_specs=VM,
-        out_shape=shape(8, 2048),
-        scratch_shapes=[pltpu.VMEM((8, 2048), F32)],
+        out_shape=jax.ShapeDtypeStruct((16, 2048), BF),
+        scratch_shapes=[pltpu.VMEM((16, 2048), F32)],
         compiler_params=limit(3),
         name="last",
-    )(*pieces, after, g2)
-    layer_out = pl.pallas_call(
-        join_kernel,
-        in_specs=[VM] * 2,
-        out_specs=VM,
-        out_shape=jax.ShapeDtypeStruct((16, 2048), BF),
-        compiler_params=limit(3),
-        name="join",
-    )(final, shifted(final, "c", 1))
+    )(both, s1, s2, s3, after, other, g2)
     return (layer_out, new_state.reshape(16, 1, 128, 128))
 
 

time: 103 us -> 95.6 us (0.928)
  waiting for transfers between devices: 26.5 us -> 11 us
  starting transfers between devices: 44.1 us -> 50.3 us
  blocking collectives: 18.7 us -> 20.1 us
    ppermute x27 -> x28, waiting for transfers between devices: 23.8 us -> 11 us  [shifted(): return lax.ppermute(value, axis, [(i, (i + step) % n) for i in range(n)])]
    ppermute x27 -> x28, starting transfers between devices: 35.5 us -> 42.1 us  [shifted(): return lax.ppermute(value, axis, [(i, (i + step) % n) for i in range(n)])]
    ppermute x1, waiting for transfers between devices: 2.69 us -> 0.01 us  [layer(): far_half = lax.ppermute(near_half, 'y', [(0, 1), (1, 0), (2, 3), (3, 2)])]
    all_to_all x1, blocking collectives: 18.7 us -> 20.1 us  [layer(): back = lax.all_to_all(partial.reshape(32, 8, 512), EP, 0, 0, tiled=True)]
  transfers between devices with their start and end apart: 29 -> 30, of which waited for: 13 -> 10; matrix products, arithmetic and copies ran while one was open for 0% -> 0% of each run, Pallas kernels for 6% -> 7%
where the time goes in v2:
time: 95.6 us; the launch traced here: 95.2 us
  starting transfers between devices  50.3 us (53%)
  blocking collectives  20.1 us (21%)
  Pallas kernels  12.9 us (13%)
  waiting for transfers between devices  11 us (12%)
    ppermute x28, starting transfers between devices, shifted(): return lax.ppermute(value, axis, [(i, (i + step) % n) for i in range(n)])  42.1 us
    all_to_all x1, blocking collectives, layer(): back = lax.all_to_all(partial.reshape(32, 8, 512), EP, 0, 0, tiled=True)  20.1 us
    ppermute x28, waiting for transfers between devices, shifted(): return lax.ppermute(value, axis, [(i, (i + step) % n) for i in range(n)])  11 us
    all_to_all x1, starting transfers between devices, layer(): block = lax.all_to_all(sent, 'z', 0, 0, tiled=True).reshape(64, 2176)  8.16 us
    pallas_call x1, Pallas kernels, layer(): pl.pallas_call(mixer_kernel, in_specs=[HB] * 16, out_specs=[VM] * 11, out...  3.45 us
    pallas_call x1, Pallas kernels, layer(): pl.pallas_call(state_kernel, in_specs=[VM, VM, HB], out_specs=HB, out_sha...  2.57 us
    pallas_call x1, Pallas kernels, layer(): pl.pallas_call(hidden_kernel, in_specs=[VM] * 7, out_specs=[VM] * 2, out_...  1.95 us
  transfers between devices with their start and end apart: 30, of which 10 were waited for; matrix products, arithmetic and copies ran while one was open for 0% of the time, Pallas kernels for 7%

profile of v2, /device:TPU:1, one launch (start us, length us, event | category | flops | bytes accessed | tf_op | source)
XLA Modules:
  0.0 95.2 jit_solution(7837104219317760719)
XLA Ops:
  0.6 0.0 copy-start
  0.7 0.0 copy-start.1
  0.7 3.4 %mixer.1 = (bf16[8,2048]{1,0:T(8,128)(2,1)S(1)}, bf16[8,2048]{1,0:T(8,128)(2,1)S(1)}, f32[16,128]{1,0:T(8,128)S(1)}, f32[16,128]{1,0:T(8,128)S(1)}, bf16[224,512...) custom-call(s32[16]{0:T(128)} %lengths.1, ...), custom_call_target="tpu_custom_call" | custom-call | tf_op jit(solution)/shard_map/mixer/pallas_call | solution.py:357
  4.1 3.3 %collective-permute-start = (bf16[8,2048]{1,0:T(8,128)(2,1)S(1)}, bf16[8,2048]{1,0:T(8,128)(2,1)S(1)}, u32[]{:S(2)}, u32[]{:S(2)}) collective-permute-start(bf16[8,2048]{1,0:T(8,128)(2,1)S(1)} %get-tuple-element.40), channel_id=1, source_target_pairs={{0,1},{1,0},{2,3},{3,2},{4,5},{5,4},{6,7},{7,6},{8,9},{9,8},{10,11... | collective-permute-start | bytes 98312 | tf_op jit(solution)/shard_map/ppermute | solution.py:26
  7.4 0.9 collective-permute-done
  8.3 0.1 collective-permute-start.1
  8.4 2.2 %collective-permute-start.2 = (bf16[8,2048]{1,0:T(8,128)(2,1)S(1)}, bf16[8,2048]{1,0:T(8,128)(2,1)S(1)}, u32[]{:S(2)}, u32[]{:S(2)}) collective-permute-start(bf16[8,2048]{1,0:T(8,128)(2,1)S(1)} %add_convert_fusion.pair), channel_id=1, source_target_pairs={{0,4},{2,6},{4,0},{6,2},{1,5},{3,7},{5,1},{7,3},{8,12},{10,14},{12... | collective-permute-start | bytes 98312 | tf_op jit(solution)/shard_map/ppermute | solution.py:26
  10.6 1.1 %collective-permute-start.3 = (bf16[8,2048]{1,0:T(8,128)(2,1)S(1)}, bf16[8,2048]{1,0:T(8,128)(2,1)S(1)}, u32[]{:S(2)}, u32[]{:S(2)}) collective-permute-start(bf16[8,2048]{1,0:T(8,128)(2,1)S(1)} %add_convert_fusion.pair), channel_id=1, source_target_pairs={{0,6},{2,0},{4,2},{6,4},{1,7},{3,1},{5,3},{7,5},{8,14},{10,8},{12,... | collective-permute-start | bytes 98312 | tf_op jit(solution)/shard_map/ppermute | solution.py:26
  11.7 0.7 collective-permute-done.1.r1
  12.4 0.8 collective-permute-done.2.r2
  13.2 0.5 collective-permute-done.3.r3
  13.7 0.9 after.1
  14.6 8.2 %all-to-all-start = ((bf16[8,8,2176]{2,1,0:T(8,128)(2,1)}), bf16[8,8,2176]{2,1,0:T(8,128)(2,1)S(1)}, u32[]{:S(2)}, u32[]{:S(2)}) async-start(bf16[8,8,2176]{2,1,0:T(8,128)(2,1)} %get-tuple-element.47), calls=%async_computation | async-start | bytes 557056 | tf_op jit(solution)/shard_map/all_to_all | solution.py:418
  22.8 3.2 %collective-permute-start.18 = (bf16[224,512]{1,0:T(8,128)(2,1)S(1)}, bf16[224,512]{1,0:T(8,128)(2,1)S(1)}, u32[]{:S(2)}, u32[]{:S(2)}) collective-permute-start(bf16[224,512]{1,0:T(8,128)(2,1)S(1)} %get-tuple-element.59), channel_id=1, source_target_pairs={{0,4},{2,6},{4,0},{6,2},{1,5},{3,7},{5,1},{7,3},{8,12},{10,14},{12... | collective-permute-start | bytes 688136 | tf_op jit(solution)/shard_map/ppermute | solution.py:26
  26.0 2.9 %collective-permute-start.10 = (bf16[32,2048]{1,0:T(8,128)(2,1)S(1)}, bf16[32,2048]{1,0:T(8,128)(2,1)S(1)}, u32[]{:S(2)}, u32[]{:S(2)}) collective-permute-start(bf16[32,2048]{1,0:T(8,128)(2,1)S(1)} %bitcast.32), channel_id=1, source_target_pairs={{0,1},{1,0},{2,3},{3,2},{4,5},{5,4},{6,7},{7,6},{8,9},{9,8},{10,11... | collective-permute-start | bytes 393224 | tf_op jit(solution)/shard_map/ppermute | solution.py:26
  28.9 0.1 collective-permute-start.11
  28.9 0.0 collective-permute-start.19
  29.0 0.9 collective-permute-done.10.refs_8_
  29.8 0.4 collective-permute-start.8
  30.2 0.2 collective-permute-start.9
  30.4 4.0 %collective-permute-start.12 = (bf16[64,2048]{1,0:T(8,128)(2,1)}, bf16[64,2048]{1,0:T(8,128)(2,1)S(1)}, u32[]{:S(2)}, u32[]{:S(2)}) collective-permute-start(bf16[64,2048]{1,0:T(8,128)(2,1)} %bitcast.27), channel_id=1, source_target_pairs={{0,1},{1,0},{2,3},{3,2},{4,5},{5,4},{6,7},{7,6},{8,9},{9,8},{10,11... | collective-permute-start | bytes 786440 | tf_op jit(solution)/shard_map/ppermute | solution.py:26
  34.4 3.0 %collective-permute-start.13 = (bf16[64,2048]{1,0:T(8,128)(2,1)}, bf16[64,2048]{1,0:T(8,128)(2,1)S(1)}, u32[]{:S(2)}, u32[]{:S(2)}) collective-permute-start(bf16[64,2048]{1,0:T(8,128)(2,1)} %bitcast.29), channel_id=1, source_target_pairs={{0,1},{1,0},{2,3},{3,2},{4,5},{5,4},{6,7},{7,6},{8,9},{9,8},{10,11... | collective-permute-start | bytes 786440 | tf_op jit(solution)/shard_map/ppermute | solution.py:26
  37.4 2.8 %collective-permute-start.6 = (bf16[32,2176]{1,0:T(8,128)(2,1)S(1)}, bf16[32,2176]{1,0:T(8,128)(2,1)S(1)}, u32[]{:S(2)}, u32[]{:S(2)}) collective-permute-start(bf16[32,2176]{1,0:T(8,128)(2,1)S(1)} %constant_dynamic-slice_fusion), channel_id=1, source_target_pairs={{0,16},{8,24},{16,0},{24,8},{1,17},{9,25},{17,1},{25,9},{2,18},{10... | collective-permute-start | bytes 417800 | tf_op jit(solution)/shard_map/ppermute | solution.py:26
  40.3 0.3 collective-permute-start.4
  40.6 3.4 %collective-permute-done.6.near_half = bf16[32,2176]{1,0:T(8,128)(2,1)S(1)} collective-permute-done((bf16[32,2176]{1,0:T(8,128)(2,1)S(1)}, bf16[32,2176]{1,0:T(8,128)(2,1)S(1)}, u32[]{:S(2)}, u32[]{:S(2)}) %collective-permute-start.6) | collective-permute-done | bytes 139296 | tf_op jit(solution)/shard_map/ppermute | solution.py:26
  44.0 2.5 %collective-permute-start.5 = (bf16[64,2176]{1,0:T(8,128)(2,1)S(1)}, bf16[64,2176]{1,0:T(8,128)(2,1)S(1)}, u32[]{:S(2)}, u32[]{:S(2)}) collective-permute-start(bf16[64,2176]{1,0:T(8,128)(2,1)S(1)} %bitcast.19), channel_id=1, source_target_pairs={{0,24},{8,0},{16,8},{24,16},{1,25},{9,1},{17,9},{25,17},{2,26},{10... | collective-permute-start | bytes 835592 | tf_op jit(solution)/shard_map/ppermute | solution.py:26
  46.5 2.1 %collective-permute-start.20 = (bf16[224,512]{1,0:T(8,128)(2,1)S(1)}, bf16[224,512]{1,0:T(8,128)(2,1)S(1)}, u32[]{:S(2)}, u32[]{:S(2)}) collective-permute-start(bf16[224,512]{1,0:T(8,128)(2,1)S(1)} %get-tuple-element.57.y0), channel_id=1, source_target_pairs={{0,1},{1,0},{2,3},{3,2},{4,5},{5,4},{6,7},{7,6},{8,9},{9,8},{10,11... | collective-permute-start | bytes 688136 | tf_op jit(solution)/shard_map/ppermute | solution.py:26
  48.6 0.1 collective-permute-start.21
  48.7 2.2 %collective-permute-start.22 = (bf16[224,512]{1,0:T(8,128)(2,1)S(1)}, bf16[224,512]{1,0:T(8,128)(2,1)S(1)}, u32[]{:S(2)}, u32[]{:S(2)}) collective-permute-start(bf16[224,512]{1,0:T(8,128)(2,1)S(1)} %collective-permute-done.18.y2), channel_id=1, source_target_pairs={{0,1},{1,0},{2,3},{3,2},{4,5},{5,4},{6,7},{7,6},{8,9},{9,8},{10,11... | collective-permute-start | bytes 688136 | tf_op jit(solution)/shard_map/ppermute | solution.py:26
  50.9 0.3 collective-permute-start.23
  51.2 1.7 %pack.1.w_all = bf16[1024,2048]{1,0:T(8,128)(2,1)S(1)} custom-call(bf16[2,64,2048]{2,1,0:T(8,128)(2,1)} %bitcast.5.refs_0_, bf16[2,64,2048]{2,1,0:T(8,128)(2,1)} %bitcast.26, bf16[32,2048]{1,0:T(8,128)(2,1)} %bitcast.31, bf16[32,2048]{1,0:T(8,128)(2,1)} %bitcast.33, bf16[64,2048]{1,0:T(8,128)(2,1)} %bitcast.28, bf16[64,2048]{1,0:T(8,128)(2,1)} %bitcast.30, ...), custom_call_target="tpu_custom_call" | custom-call | tf_op jit(solution)/shard_map/pack/pallas_call | solution.py:425
  52.9 1.9 %hidden.1 = (bf16[272,128]{1,0:T(8,128)(2,1)S(1)}, bf16[256,128]{1,0:T(8,128)(2,1)S(1)}) custom-call(bf16[64,2176]{1,0:T(8,128)(2,1)S(1)} %bitcast.20, bf16[64,2176]{1,0:T(8,128)(2,1)S(1)} %collective-permute-done.4.b1, bf16[64,2176]{1,0:T(8,128)(2,1)S(1)} %collective-permute-done.5.b3, bf16[32,2176]{1,0:T(8,128)(2,1)S(1)} %collective-permute-done.6.near_half, ...), custom_call_target="tpu_custom_call" | custom-call | tf_op jit(solution)/shard_map/hidden/pallas_call | solution.py:448
  54.9 0.7 collective-permute-start.14
  55.6 2.9 %collective-permute-start.15 = (bf16[272,128]{1,0:T(8,128)(2,1)S(1)}, bf16[272,128]{1,0:T(8,128)(2,1)S(1)}, u32[]{:S(2)}, u32[]{:S(2)}) collective-permute-start(bf16[272,128]{1,0:T(8,128)(2,1)S(1)} %get-tuple-element.55.h0), channel_id=1, source_target_pairs={{0,4},{2,6},{4,0},{6,2},{1,5},{3,7},{5,1},{7,3},{8,12},{10,14},{12... | collective-permute-start | bytes 208904 | tf_op jit(solution)/shard_map/ppermute | solution.py:26
  58.4 0.1 collective-permute-start.16
  58.6 0.7 arrange.1
  59.3 2.3 %collective-permute-done.15.h2 = bf16[272,128]{1,0:T(8,128)(2,1)S(1)} collective-permute-done((bf16[272,128]{1,0:T(8,128)(2,1)S(1)}, bf16[272,128]{1,0:T(8,128)(2,1)S(1)}, u32[]{:S(2)}, u32[]{:S(2)}) %collective-permute-start.15) | collective-permute-done | bytes 69664 | tf_op jit(solution)/shard_map/ppermute | solution.py:26
  61.6 0.7 collective-permute-done.16.h3
  62.3 0.7 down.1
  63.0 20.1 %all_to_all.10.back = bf16[32,8,512]{2,1,0:T(8,128)(2,1)S(1)} all-to-all(bf16[32,8,512]{2,1,0:T(8,128)(2,1)S(1)} %bitcast.21), channel_id=1, replica_groups=mesh['z'=8,'x'=4,'y'=4,'c'=2] {'z','x'}, dimensions={0} | all-to-all | bytes 524288 | tf_op jit(solution)/shard_map/all_to_all | solution.py:482
  83.2 3.8 %collective-permute-start.24 = (f32[8,512]{1,0:T(8,128)S(1)}, f32[8,512]{1,0:T(8,128)S(1)}, u32[]{:S(2)}, u32[]{:S(2)}) collective-permute-start(f32[8,512]{1,0:T(8,128)S(1)} %sum.1.own), channel_id=1, source_target_pairs={{0,1},{1,0},{2,3},{3,2},{4,5},{5,4},{6,7},{7,6},{8,9},{9,8},{10,11... | collective-permute-start | bytes 49160 | tf_op jit(solution)/shard_map/ppermute | solution.py:26
  87.0 0.1 collective-permute-start.28
  87.1 0.7 collective-permute-done.24.other
  87.9 0.6 collective-permute-start.25
  88.4 3.2 %collective-permute-start.26 = (f32[16,512]{1,0:T(8,128)S(1)}, f32[16,512]{1,0:T(8,128)S(1)}, u32[]{:S(2)}, u32[]{:S(2)}) collective-permute-start(f32[16,512]{1,0:T(8,128)S(1)} %both.1.s0), channel_id=1, source_target_pairs={{0,4},{2,6},{4,0},{6,2},{1,5},{3,7},{5,1},{7,3},{8,12},{10,14},{12... | collective-permute-start | bytes 98312 | tf_op jit(solution)/shard_map/ppermute | solution.py:26
  91.6 2.6 %state.1 = f32[16,128,128]{2,1,0:T(8,128)} custom-call(f32[16,128]{1,0:T(8,128)S(1)} %get-tuple-element.66.keys, f32[16,128]{1,0:T(8,128)S(1)} %get-tuple-element.67.values, f32[16,128,128]{2,1,0:T(8,128)} %bitcast.23), custom_call_target="tpu_custom_call" | custom-call | tf_op jit(solution)/shard_map/state/pallas_call | solution.py:434
  94.2 0.2 collective-permute-done.27.s3
  94.4 0.9 last.1
  (32 shorter events, 0.2 us)
Async XLA Ops:
  0.6 7.7 %copy-start.2 = (bf16[2048]{0:T(1024)(128)(2,1)S(1)}, bf16[2048]{0:T(1024)(128)(2,1)}, u32[]{:S(2)}) copy-start(bf16[2048]{0:T(1024)(128)(2,1)} %param.42) | copy-start | bytes 12292
  0.6 25.3 %copy-start = (bf16[2048,32]{0,1:T(8,128)(2,1)S(1)}, bf16[2048,32]{0,1:T(8,128)(2,1)}, u32[]{:S(2)}) copy-start(bf16[2048,32]{0,1:T(8,128)(2,1)} %param.43) | copy-start | bytes 393220
  0.7 28.2 %copy-start.1 = (bf16[2048,32]{0,1:T(8,128)(2,1)S(1)}, bf16[2048,32]{0,1:T(8,128)(2,1)}, u32[]{:S(2)}) copy-start(bf16[2048,32]{0,1:T(8,128)(2,1)} %param.44) | copy-start | bytes 393220
  4.1 4.1 %collective-permute-start = (bf16[8,2048]{1,0:T(8,128)(2,1)S(1)}, bf16[8,2048]{1,0:T(8,128)(2,1)S(1)}, u32[]{:S(2)}, u32[]{:S(2)}) collective-permute-start(bf16[8,2048]{1,0:T(8,128)(2,1)S(1)} %get-tuple-element.40), channel_id=1, source_target_pairs={{0,1},{1,0},{2,3},{3,2},{4,5},{5,4},{6,7},{7,6},{8,9},{9,8},{10,11... | collective-permute-start | bytes 98312 | tf_op jit(solution)/shard_map/ppermute | solution.py:26
  8.3 4.1 %collective-permute-start.1 = (bf16[8,2048]{1,0:T(8,128)(2,1)S(1)}, bf16[8,2048]{1,0:T(8,128)(2,1)S(1)}, u32[]{:S(2)}, u32[]{:S(2)}) collective-permute-start(bf16[8,2048]{1,0:T(8,128)(2,1)S(1)} %add_convert_fusion.pair), channel_id=1, source_target_pairs={{0,2},{2,4},{4,6},{6,0},{1,3},{3,5},{5,7},{7,1},{8,10},{10,12},{12... | collective-permute-start | bytes 98312 | tf_op jit(solution)/shard_map/ppermute | solution.py:26
  8.4 4.8 %collective-permute-start.2 = (bf16[8,2048]{1,0:T(8,128)(2,1)S(1)}, bf16[8,2048]{1,0:T(8,128)(2,1)S(1)}, u32[]{:S(2)}, u32[]{:S(2)}) collective-permute-start(bf16[8,2048]{1,0:T(8,128)(2,1)S(1)} %add_convert_fusion.pair), channel_id=1, source_target_pairs={{0,4},{2,6},{4,0},{6,2},{1,5},{3,7},{5,1},{7,3},{8,12},{10,14},{12... | collective-permute-start | bytes 98312 | tf_op jit(solution)/shard_map/ppermute | solution.py:26
  10.6 3.1 %collective-permute-start.3 = (bf16[8,2048]{1,0:T(8,128)(2,1)S(1)}, bf16[8,2048]{1,0:T(8,128)(2,1)S(1)}, u32[]{:S(2)}, u32[]{:S(2)}) collective-permute-start(bf16[8,2048]{1,0:T(8,128)(2,1)S(1)} %add_convert_fusion.pair), channel_id=1, source_target_pairs={{0,6},{2,0},{4,2},{6,4},{1,7},{3,1},{5,3},{7,5},{8,14},{10,8},{12,... | collective-permute-start | bytes 98312 | tf_op jit(solution)/shard_map/ppermute | solution.py:26
  14.6 22.8 %all-to-all-start = ((bf16[8,8,2176]{2,1,0:T(8,128)(2,1)}), bf16[8,8,2176]{2,1,0:T(8,128)(2,1)S(1)}, u32[]{:S(2)}, u32[]{:S(2)}) async-start(bf16[8,8,2176]{2,1,0:T(8,128)(2,1)} %get-tuple-element.47), calls=%async_computation | async-start | bytes 557056 | tf_op jit(solution)/shard_map/all_to_all | solution.py:418
  22.8 7.6 %collective-permute-start.17 = (bf16[224,512]{1,0:T(8,128)(2,1)S(1)}, bf16[224,512]{1,0:T(8,128)(2,1)S(1)}, u32[]{:S(2)}, u32[]{:S(2)}) collective-permute-start(bf16[224,512]{1,0:T(8,128)(2,1)S(1)} %get-tuple-element.58), channel_id=1, source_target_pairs={{0,2},{2,4},{4,6},{6,0},{1,3},{3,5},{5,7},{7,1},{8,10},{10,12},{12... | collective-permute-start | bytes 688136 | tf_op jit(solution)/shard_map/ppermute | solution.py:26
  22.8 11.6 %collective-permute-start.18 = (bf16[224,512]{1,0:T(8,128)(2,1)S(1)}, bf16[224,512]{1,0:T(8,128)(2,1)S(1)}, u32[]{:S(2)}, u32[]{:S(2)}) collective-permute-start(bf16[224,512]{1,0:T(8,128)(2,1)S(1)} %get-tuple-element.59), channel_id=1, source_target_pairs={{0,4},{2,6},{4,0},{6,2},{1,5},{3,7},{5,1},{7,3},{8,12},{10,14},{12... | collective-permute-start | bytes 688136 | tf_op jit(solution)/shard_map/ppermute | solution.py:26
  26.0 3.9 %collective-permute-start.10 = (bf16[32,2048]{1,0:T(8,128)(2,1)S(1)}, bf16[32,2048]{1,0:T(8,128)(2,1)S(1)}, u32[]{:S(2)}, u32[]{:S(2)}) collective-permute-start(bf16[32,2048]{1,0:T(8,128)(2,1)S(1)} %bitcast.32), channel_id=1, source_target_pairs={{0,1},{1,0},{2,3},{3,2},{4,5},{5,4},{6,7},{7,6},{8,9},{9,8},{10,11... | collective-permute-start | bytes 393224 | tf_op jit(solution)/shard_map/ppermute | solution.py:26
  28.9 1.3 %collective-permute-start.11 = (bf16[32,2048]{1,0:T(8,128)(2,1)S(1)}, bf16[32,2048]{1,0:T(8,128)(2,1)S(1)}, u32[]{:S(2)}, u32[]{:S(2)}) collective-permute-start(bf16[32,2048]{1,0:T(8,128)(2,1)S(1)} %bitcast.34), channel_id=1, source_target_pairs={{0,1},{1,0},{2,3},{3,2},{4,5},{5,4},{6,7},{7,6},{8,9},{9,8},{10,11... | collective-permute-start | bytes 393224 | tf_op jit(solution)/shard_map/ppermute | solution.py:26
  28.9 8.5 %collective-permute-start.19 = (bf16[224,512]{1,0:T(8,128)(2,1)S(1)}, bf16[224,512]{1,0:T(8,128)(2,1)S(1)}, u32[]{:S(2)}, u32[]{:S(2)}) collective-permute-start(bf16[224,512]{1,0:T(8,128)(2,1)S(1)} %get-tuple-element.60), channel_id=1, source_target_pairs={{0,6},{2,0},{4,2},{6,4},{1,7},{3,1},{5,3},{7,5},{8,14},{10,8},{12,... | collective-permute-start | bytes 688136 | tf_op jit(solution)/shard_map/ppermute | solution.py:26
  29.8 16.6 %collective-permute-start.8 = (bf16[2,64,2048]{2,1,0:T(8,128)(2,1)}, bf16[2,64,2048]{2,1,0:T(8,128)(2,1)S(1)}, u32[]{:S(2)}, u32[]{:S(2)}) collective-permute-start(bf16[2,64,2048]{2,1,0:T(8,128)(2,1)} %bitcast.5.refs_0_), channel_id=1, source_target_pairs={{0,1},{1,0},{2,3},{3,2},{4,5},{5,4},{6,7},{7,6},{8,9},{9,8},{10,11... | collective-permute-start | bytes 1572872 | tf_op jit(solution)/shard_map/ppermute | solution.py:26
  30.2 18.4 %collective-permute-start.9 = (bf16[2,64,2048]{2,1,0:T(8,128)(2,1)}, bf16[2,64,2048]{2,1,0:T(8,128)(2,1)S(1)}, u32[]{:S(2)}, u32[]{:S(2)}) collective-permute-start(bf16[2,64,2048]{2,1,0:T(8,128)(2,1)} %bitcast.25), channel_id=1, source_target_pairs={{0,1},{1,0},{2,3},{3,2},{4,5},{5,4},{6,7},{7,6},{8,9},{9,8},{10,11... | collective-permute-start | bytes 1572872 | tf_op jit(solution)/shard_map/ppermute | solution.py:26
  30.4 9.9 %collective-permute-start.12 = (bf16[64,2048]{1,0:T(8,128)(2,1)}, bf16[64,2048]{1,0:T(8,128)(2,1)S(1)}, u32[]{:S(2)}, u32[]{:S(2)}) collective-permute-start(bf16[64,2048]{1,0:T(8,128)(2,1)} %bitcast.27), channel_id=1, source_target_pairs={{0,1},{1,0},{2,3},{3,2},{4,5},{5,4},{6,7},{7,6},{8,9},{9,8},{10,11... | collective-permute-start | bytes 786440 | tf_op jit(solution)/shard_map/ppermute | solution.py:26
  34.4 9.6 %collective-permute-start.13 = (bf16[64,2048]{1,0:T(8,128)(2,1)}, bf16[64,2048]{1,0:T(8,128)(2,1)S(1)}, u32[]{:S(2)}, u32[]{:S(2)}) collective-permute-start(bf16[64,2048]{1,0:T(8,128)(2,1)} %bitcast.29), channel_id=1, source_target_pairs={{0,1},{1,0},{2,3},{3,2},{4,5},{5,4},{6,7},{7,6},{8,9},{9,8},{10,11... | collective-permute-start | bytes 786440 | tf_op jit(solution)/shard_map/ppermute | solution.py:26
  37.4 6.5 %collective-permute-start.6 = (bf16[32,2176]{1,0:T(8,128)(2,1)S(1)}, bf16[32,2176]{1,0:T(8,128)(2,1)S(1)}, u32[]{:S(2)}, u32[]{:S(2)}) collective-permute-start(bf16[32,2176]{1,0:T(8,128)(2,1)S(1)} %constant_dynamic-slice_fusion), channel_id=1, source_target_pairs={{0,16},{8,24},{16,0},{24,8},{1,17},{9,25},{17,1},{25,9},{2,18},{10... | collective-permute-start | bytes 417800 | tf_op jit(solution)/shard_map/ppermute | solution.py:26
  40.3 10.7 %collective-permute-start.4 = (bf16[64,2176]{1,0:T(8,128)(2,1)S(1)}, bf16[64,2176]{1,0:T(8,128)(2,1)S(1)}, u32[]{:S(2)}, u32[]{:S(2)}) collective-permute-start(bf16[64,2176]{1,0:T(8,128)(2,1)S(1)} %bitcast.18), channel_id=1, source_target_pairs={{0,8},{8,16},{16,24},{24,0},{1,9},{9,17},{17,25},{25,1},{2,10},{10... | collective-permute-start | bytes 835592 | tf_op jit(solution)/shard_map/ppermute | solution.py:26
  44.0 4.7 %collective-permute-start.7 = (bf16[32,2176]{1,0:T(8,128)(2,1)S(1)}, bf16[32,2176]{1,0:T(8,128)(2,1)S(1)}, u32[]{:S(2)}, u32[]{:S(2)}) collective-permute-start(bf16[32,2176]{1,0:T(8,128)(2,1)S(1)} %collective-permute-done.6.near_half), channel_id=1, source_target_pairs={{0,2},{2,0},{4,6},{6,4},{1,3},{3,1},{5,7},{7,5},{8,10},{10,8},{12,... | collective-permute-start | bytes 417800 | tf_op jit(solution)/shard_map/ppermute | solution.py:422
  44.0 8.9 %collective-permute-start.5 = (bf16[64,2176]{1,0:T(8,128)(2,1)S(1)}, bf16[64,2176]{1,0:T(8,128)(2,1)S(1)}, u32[]{:S(2)}, u32[]{:S(2)}) collective-permute-start(bf16[64,2176]{1,0:T(8,128)(2,1)S(1)} %bitcast.19), channel_id=1, source_target_pairs={{0,24},{8,0},{16,8},{24,16},{1,25},{9,1},{17,9},{25,17},{2,26},{10... | collective-permute-start | bytes 835592 | tf_op jit(solution)/shard_map/ppermute | solution.py:26
  46.5 9.1 %collective-permute-start.20 = (bf16[224,512]{1,0:T(8,128)(2,1)S(1)}, bf16[224,512]{1,0:T(8,128)(2,1)S(1)}, u32[]{:S(2)}, u32[]{:S(2)}) collective-permute-start(bf16[224,512]{1,0:T(8,128)(2,1)S(1)} %get-tuple-element.57.y0), channel_id=1, source_target_pairs={{0,1},{1,0},{2,3},{3,2},{4,5},{5,4},{6,7},{7,6},{8,9},{9,8},{10,11... | collective-permute-start | bytes 688136 | tf_op jit(solution)/shard_map/ppermute | solution.py:26
  48.6 9.9 %collective-permute-start.21 = (bf16[224,512]{1,0:T(8,128)(2,1)S(1)}, bf16[224,512]{1,0:T(8,128)(2,1)S(1)}, u32[]{:S(2)}, u32[]{:S(2)}) collective-permute-start(bf16[224,512]{1,0:T(8,128)(2,1)S(1)} %collective-permute-done.17.y1), channel_id=1, source_target_pairs={{0,1},{1,0},{2,3},{3,2},{4,5},{5,4},{6,7},{7,6},{8,9},{9,8},{10,11... | collective-permute-start | bytes 688136 | tf_op jit(solution)/shard_map/ppermute | solution.py:26
  48.7 9.9 %collective-permute-start.22 = (bf16[224,512]{1,0:T(8,128)(2,1)S(1)}, bf16[224,512]{1,0:T(8,128)(2,1)S(1)}, u32[]{:S(2)}, u32[]{:S(2)}) collective-permute-start(bf16[224,512]{1,0:T(8,128)(2,1)S(1)} %collective-permute-done.18.y2), channel_id=1, source_target_pairs={{0,1},{1,0},{2,3},{3,2},{4,5},{5,4},{6,7},{7,6},{8,9},{9,8},{10,11... | collective-permute-start | bytes 688136 | tf_op jit(solution)/shard_map/ppermute | solution.py:26
  50.9 7.7 %collective-permute-start.23 = (bf16[224,512]{1,0:T(8,128)(2,1)S(1)}, bf16[224,512]{1,0:T(8,128)(2,1)S(1)}, u32[]{:S(2)}, u32[]{:S(2)}) collective-permute-start(bf16[224,512]{1,0:T(8,128)(2,1)S(1)} %collective-permute-done.19.y3), channel_id=1, source_target_pairs={{0,1},{1,0},{2,3},{3,2},{4,5},{5,4},{6,7},{7,6},{8,9},{9,8},{10,11... | collective-permute-start | bytes 688136 | tf_op jit(solution)/shard_map/ppermute | solution.py:26
  54.9 4.4 %collective-permute-start.14 = (bf16[272,128]{1,0:T(8,128)(2,1)S(1)}, bf16[272,128]{1,0:T(8,128)(2,1)S(1)}, u32[]{:S(2)}, u32[]{:S(2)}) collective-permute-start(bf16[272,128]{1,0:T(8,128)(2,1)S(1)} %get-tuple-element.55.h0), channel_id=1, source_target_pairs={{0,2},{2,4},{4,6},{6,0},{1,3},{3,5},{5,7},{7,1},{8,10},{10,12},{12... | collective-permute-start | bytes 208904 | tf_op jit(solution)/shard_map/ppermute | solution.py:26
  55.6 6.0 %collective-permute-start.15 = (bf16[272,128]{1,0:T(8,128)(2,1)S(1)}, bf16[272,128]{1,0:T(8,128)(2,1)S(1)}, u32[]{:S(2)}, u32[]{:S(2)}) collective-permute-start(bf16[272,128]{1,0:T(8,128)(2,1)S(1)} %get-tuple-element.55.h0), channel_id=1, source_target_pairs={{0,4},{2,6},{4,0},{6,2},{1,5},{3,7},{5,1},{7,3},{8,12},{10,14},{12... | collective-permute-start | bytes 208904 | tf_op jit(solution)/shard_map/ppermute | solution.py:26
  58.4 3.9 %collective-permute-start.16 = (bf16[272,128]{1,0:T(8,128)(2,1)S(1)}, bf16[272,128]{1,0:T(8,128)(2,1)S(1)}, u32[]{:S(2)}, u32[]{:S(2)}) collective-permute-start(bf16[272,128]{1,0:T(8,128)(2,1)S(1)} %get-tuple-element.55.h0), channel_id=1, source_target_pairs={{0,6},{2,0},{4,2},{6,4},{1,7},{3,1},{5,3},{7,5},{8,14},{10,8},{12,... | collective-permute-start | bytes 208904 | tf_op jit(solution)/shard_map/ppermute | solution.py:26
  83.2 4.7 %collective-permute-start.24 = (f32[8,512]{1,0:T(8,128)S(1)}, f32[8,512]{1,0:T(8,128)S(1)}, u32[]{:S(2)}, u32[]{:S(2)}) collective-permute-start(f32[8,512]{1,0:T(8,128)S(1)} %sum.1.own), channel_id=1, source_target_pairs={{0,1},{1,0},{2,3},{3,2},{4,5},{5,4},{6,7},{7,6},{8,9},{9,8},{10,11... | collective-permute-start | bytes 49160 | tf_op jit(solution)/shard_map/ppermute | solution.py:26
  87.0 7.2 %collective-permute-start.28 = (bf16[8,2048]{1,0:T(8,128)(2,1)S(1)}, bf16[8,2048]{1,0:T(8,128)(2,1)S(1)}, u32[]{:S(2)}, u32[]{:S(2)}) collective-permute-start(bf16[8,2048]{1,0:T(8,128)(2,1)S(1)} %get-tuple-element.64.own), channel_id=1, source_target_pairs={{0,1},{1,0},{2,3},{3,2},{4,5},{5,4},{6,7},{7,6},{8,9},{9,8},{10,11... | collective-permute-start | bytes 98312 | tf_op jit(solution)/shard_map/ppermute | solution.py:26
  87.9 6.3 %collective-permute-start.25 = (f32[16,512]{1,0:T(8,128)S(1)}, f32[16,512]{1,0:T(8,128)S(1)}, u32[]{:S(2)}, u32[]{:S(2)}) collective-permute-start(f32[16,512]{1,0:T(8,128)S(1)} %both.1.s0), channel_id=1, source_target_pairs={{0,2},{2,4},{4,6},{6,0},{1,3},{3,5},{5,7},{7,1},{8,10},{10,12},{12... | collective-permute-start | bytes 98312 | tf_op jit(solution)/shard_map/ppermute | solution.py:26
  88.4 5.8 %collective-permute-start.26 = (f32[16,512]{1,0:T(8,128)S(1)}, f32[16,512]{1,0:T(8,128)S(1)}, u32[]{:S(2)}, u32[]{:S(2)}) collective-permute-start(f32[16,512]{1,0:T(8,128)S(1)} %both.1.s0), channel_id=1, source_target_pairs={{0,4},{2,6},{4,0},{6,2},{1,5},{3,7},{5,1},{7,3},{8,12},{10,14},{12... | collective-permute-start | bytes 98312 | tf_op jit(solution)/shard_map/ppermute | solution.py:26
  91.6 2.8 %collective-permute-start.27 = (f32[16,512]{1,0:T(8,128)S(1)}, f32[16,512]{1,0:T(8,128)S(1)}, u32[]{:S(2)}, u32[]{:S(2)}) collective-permute-start(f32[16,512]{1,0:T(8,128)S(1)} %both.1.s0), channel_id=1, source_target_pairs={{0,6},{2,0},{4,2},{6,4},{1,7},{3,1},{5,3},{7,5},{8,14},{10,8},{12,... | collective-permute-start | bytes 98312 | tf_op jit(solution)/shard_map/ppermute | solution.py:26
